TPU v7x, 128 devices: a whole 4x4x4 slice. The times are simulated.
128 devices in a mesh: sp: 64 (over z, y, x), tp: 2 (over core).
Axes of the slice: x: 4, y: 4, z: 4, core: 2. Of those that a mesh axis runs over, the one named last changes fastest.
Arguments:
- stream: bfloat16 [16384, 2048], P('sp', 'tp'), may hold values from -6 to 6
- out_grad: bfloat16 [16384, 2048], P('sp', 'tp'), may hold values from -16 to 16
- gate_in: bfloat16 [16384, 1024], P('sp', 'tp'), may hold values from -6 to 6
- conv_gate: bfloat16 [16384, 1024], P('sp', 'tp'), may hold values from -6 to 6
- conv_value: bfloat16 [16384, 1024], P('sp', 'tp'), may hold values from -6 to 6
- taps: float32 [3, 1024], P(None, 'tp'), may hold values from -3.5 to 3.5
- w_out: bfloat16 [2048, 1024], P(None, 'tp'), may hold values from -0.1875 to 0.1875
- route_ids: int32 [16384, 2], P('sp'), may hold values from 0 to 63, all different within a row; in each aligned block of 256 rows (0 to 255, 256 to 511, ...) at most 16 rows name the same one
- route_weights: float32 [16384, 2], P('sp'), may hold values from 0.1 to 1
- w_gate: bfloat16 [64, 2048, 1024], P('sp', None, 'tp'), may hold values from -0.125 to 0.125
- w_up: bfloat16 [64, 2048, 1024], P('sp', None, 'tp'), may hold values from -0.125 to 0.125
- w_down: bfloat16 [64, 1024, 2048], P('sp', 'tp'), may hold values from -0.1875 to 0.1875
Outputs:
- stream_grad: bfloat16 [16384, 2048], P('sp', 'tp')
- gate_in_grad: bfloat16 [16384, 1024], P('sp', 'tp')
- conv_gate_grad: bfloat16 [16384, 1024], P('sp', 'tp')
- conv_value_grad: bfloat16 [16384, 1024], P('sp', 'tp')
- w_out_grad: float32 [2048, 1024], P('sp', 'tp')
- w_gate_grad: float32 [64, 2048, 1024], P('sp', None, 'tp')
- w_up_grad: float32 [64, 2048, 1024], P('sp', None, 'tp')
- w_down_grad: float32 [64, 1024, 2048], P('sp', 'tp')
Inputs may be any that keep to these rules, and one draw needn't show every extreme that they name: `route_ids`: the ids of one token differ. Within each aligned block of 256 tokens (the rows of one index of sp), no expert is named by more than 16 routes, and in every draw some expert is named by exactly 16 routes of some block.
All inputs are finite; a program needn't handle non-finite values.
Results may differ from a plain program's by a relative error of at most 0.009.
Values may be sent and summed in bfloat16 or wider, within the bound.
A program may use at most 128 MiB of HBM per device.

v0:
```python
import functools

import jax
import jax.numpy as jnp
from jax import lax
from jax.experimental import pallas as pl
from jax.experimental.pallas import tpu as pltpu
from jax.sharding import PartitionSpec as P

MESH = pl.DeviceIdType.MESH
BF = jnp.bfloat16
F32 = jnp.float32
SIDE = 4
SLOTS = 16
STRIDE = (16, 4, 1)
ORDERS = ((2, 1, 0), (1, 0, 2), (0, 2, 1))
X_CUTS = ((0, 384), (384, 384), (768, 256))
G_CUTS = ((0, 256), (256, 384), (640, 384))


def coordinate(dim):
    return (lax.axis_index("sp") // STRIDE[dim]) % SIDE


def peer_of(dim, by):
    here = coordinate(dim)
    return lax.axis_index("sp") + ((here + by) % SIDE - here) * STRIDE[dim]


def piece(spot, dim, at, width):
    ref, start = spot
    index = [slice(None)] * 3
    index[dim] = at
    return ref.at[(*index, slice(None), pl.ds(start, width))]


def phase_copies(source, target, dim, width, send_sem, recv_sem, local_sem):
    here = coordinate(dim)
    tp = lax.axis_index("tp")
    copies = []
    for by in (2, 1, 3):
        copies.append(
            pltpu.make_async_remote_copy(
                src_ref=piece(source, dim, (here + by) % SIDE, width),
                dst_ref=piece(target, dim, here, width),
                send_sem=send_sem.at[by - 1],
                recv_sem=recv_sem.at[by - 1],
                device_id=(peer_of(dim, by), tp),
                device_id_type=MESH,
            )
        )
    copies.append(
        pltpu.make_async_copy(
            piece(source, dim, here, width), piece(target, dim, here, width), local_sem
        )
    )
    return copies


def start_all(copies):
    for copy in copies:
        copy.start()


def arrive_all(copies):
    for copy in copies[:-1]:
        copy.wait_recv()
    copies[-1].wait()


def slots_in_lanes(ids):
    tokens = ids.shape[1]
    expert = lax.broadcasted_iota(jnp.int32, (64, tokens), 0)
    first, second = ids[0:1, :], ids[1:2, :]
    named = jnp.where((expert == first) | (expert == second), 1.0, 0.0)
    before = (
        lax.broadcasted_iota(jnp.int32, (tokens, tokens), 0)
        < lax.broadcasted_iota(jnp.int32, (tokens, tokens), 1)
    )
    earlier = jnp.dot(
        named.astype(BF), jnp.where(before, 1.0, 0.0).astype(BF), preferred_element_type=F32
    )
    position = [
        jnp.sum(jnp.where(expert == which, earlier, 0.0), axis=0, keepdims=True).astype(jnp.int32)
        for which in (first, second)
    ]
    return first * SLOTS + position[0], second * SLOTS + position[1]


UNIT_CUTS = ((0, 3), (3, 3), (6, 2))


def greet_all():
    barrier = pltpu.get_barrier_semaphore()
    tp = lax.axis_index("tp")
    sp = lax.axis_index("sp")
    for dim in range(3):
        for by in range(1, SIDE):
            pl.semaphore_signal(
                barrier, inc=1, device_id=(peer_of(dim, by), tp), device_id_type=MESH
            )
    for other in ((sp, 1 - tp), ((sp + 1) % 64, tp), ((sp + 63) % 64, tp)):
        pl.semaphore_signal(barrier, inc=1, device_id=other, device_id_type=MESH)


def all_greeted():
    pl.semaphore_wait(pltpu.get_barrier_semaphore(), 12)


def remote(source, target, send_sem, recv_sem, device):
    return pltpu.make_async_remote_copy(
        src_ref=source,
        dst_ref=target,
        send_sem=send_sem,
        recv_sem=recv_sem,
        device_id=device,
        device_id_type=MESH,
    )


def dot(a, b):
    return jnp.dot(a, b, preferred_element_type=F32)


def dot_tn(a, b):
    return lax.dot_general(a, b, (((0,), (0,)), ((), ())), preferred_element_type=F32)


def dot_nt(a, b):
    return lax.dot_general(a, b, (((1,), (1,)), ((), ())), preferred_element_type=F32)


def main_kernel(
    ids_ref,
    weights_ref,
    stream_ref,
    cot_ref,
    gate_in_ref,
    conv_gate_ref,
    conv_value_ref,
    taps_ref,
    w_out_hbm,
    w_gate_hbm,
    w_up_hbm,
    w_down_hbm,
    half_ref,
    gate_in_grad_ref,
    conv_gate_grad_ref,
    conv_value_grad_ref,
    out_block_ref,
    x_hbm,
    g_hbm,
    hidden_hbm,
    gate_hbm,
    up_hbm,
    send,
    middle,
    full_x,
    full_g,
    wg,
    wu,
    wd,
    w_out,
    silu_keep,
    slope_keep,
    hidden,
    gate_grad,
    up_grad,
    arrived,
    back,
    hot_ref,
    whole,
    blocks,
    got1,
    sum1,
    got2,
    sum2,
    got3,
    pad_left,
    pad_right,
    halo,
    conv_sum_ref,
    mixer_out,
    load_sems,
    save_sems,
    send_sems,
    recv_sems,
    local_sems,
    tp_send,
    tp_recv,
    halo_send,
    halo_recv,
    fold_send,
    fold_recv,
):
    tp = lax.axis_index("tp")
    sp = lax.axis_index("sp")
    partner = (sp, 1 - tp)
    greet_all()
    loads = [
        pltpu.make_async_copy(source, target, load_sems.at[k])
        for k, (source, target) in enumerate(
            ((w_gate_hbm.at[0], wg), (w_up_hbm.at[0], wu), (w_down_hbm.at[0], wd), (w_out_hbm, w_out))
        )
    ]
    start_all(loads)

    slot0, slot1 = slots_in_lanes(ids_ref[...])
    weight0, weight1 = weights_ref[0:1, :], weights_ref[1:2, :]
    for z in range(SIDE):
        row = lax.broadcasted_iota(jnp.int32, (256, 256), 0) + z * 256
        hot = jnp.where((row == slot0) | (row == slot1), 1.0, 0.0).astype(BF)
        hot_ref[pl.ds(z * 256, 256), :] = hot
        send[0, z] = dot(hot, stream_ref[...]).astype(BF).reshape(4, 4, SLOTS, 1024)

    def own_half(ref, cut):
        start = pl.multiple_of(tp * 1024 + cut[0], 128)
        return ref.at[:, :, :, :, pl.ds(start, cut[1])]

    full = (full_x, full_g)
    portions = []
    for tensor, cuts in enumerate((X_CUTS, G_CUTS)):
        for which, cut in enumerate(cuts):
            number = tensor * 3 + which
            spots = [
                (send.at[tensor], cut[0]),
                (middle.at[0, tensor], cut[0]),
                (middle.at[1, tensor], cut[0]),
                (full[tensor], pl.multiple_of(tp * 1024 + cut[0], 128)),
            ]
            portions.append(
                [
                    phase_copies(
                        spots[phase],
                        spots[phase + 1],
                        ORDERS[which][phase],
                        cut[1],
                        send_sems.at[number, phase],
                        recv_sems.at[number, phase],
                        local_sems.at[number, phase],
                    )
                    for phase in range(3)
                ]
            )
    all_greeted()
    for portion in portions[:3]:
        start_all(portion[0])
    for z in range(SIDE):
        row = lax.broadcasted_iota(jnp.int32, (256, 256), 0) + z * 256
        scale = jnp.sum(
            jnp.where(row == slot0, weight0, 0.0) + jnp.where(row == slot1, weight1, 0.0),
            axis=1,
            keepdims=True,
        )
        hot = hot_ref[pl.ds(z * 256, 256), :]
        send[1, z] = (scale * dot(hot, cot_ref[...])).astype(BF).reshape(4, 4, SLOTS, 1024)
    for portion in portions[3:]:
        start_all(portion[0])

    pad_left[pl.ds(8, 256), :] = conv_gate_ref[...].astype(F32) * conv_value_ref[...].astype(F32)
    left = remote(
        pad_left.at[pl.ds(256, 8)],
        halo.at[0],
        halo_send.at[0],
        halo_recv.at[0],
        ((sp + 1) % 64, tp),
    )
    left.start()
    for portion in portions:
        arrive_all(portion[0])
        start_all(portion[1])
    left.wait()
    pad_left[pl.ds(0, 8), :] = jnp.where(sp == 0, 0.0, halo[0])
    conv_sum = jnp.zeros((256, 512), F32)
    for tap in range(3):
        conv_sum = conv_sum + taps_ref[tap : tap + 1, :] * pad_left[pl.ds(6 + tap, 256), :]
    conv_sum_ref[...] = conv_sum
    mixer_out[...] = (gate_in_ref[...].astype(F32) * conv_sum).astype(BF)
    for portion in portions:
        arrive_all(portion[1])
        start_all(portion[2])

    crossings = []
    saves = []

    def cross(tensor):
        for which, cut in enumerate((X_CUTS, G_CUTS)[tensor]):
            number = tensor * 3 + which
            arrive_all(portions[number][2])
            part = own_half(full[tensor], cut)
            crossing = remote(part, part, tp_send.at[number], tp_recv.at[number], partner)
            crossing.start()
            crossings.append(crossing)

    def save(source, target):
        copy = pltpu.make_async_copy(source, target, save_sems.at[len(saves)])
        copy.start()
        saves.append(copy)

    cross(0)
    for load in loads:
        load.wait()
    for crossing in crossings[:3]:
        crossing.wait()

    def activate(step, carry):
        rows = full_x[pl.ds(step * 2, 2)].reshape(512, 2048)
        at = pl.ds(pl.multiple_of(step * 512, 512), 512)
        pre_gate = dot(rows, wg[...])
        pre_up = dot(rows, wu[...])
        sigmoid = jax.nn.sigmoid(pre_gate)
        silu = pre_gate * sigmoid
        silu_keep[at, :] = silu
        slope_keep[at, :] = pre_up * sigmoid * (1.0 + pre_gate * (1.0 - sigmoid))
        hidden[at, :] = (silu * pre_up).astype(BF)
        return carry

    lax.fori_loop(0, 2, activate, 0)
    save(full_x, x_hbm)
    save(hidden, hidden_hbm)
    cross(1)
    for crossing in crossings[3:]:
        crossing.wait()

    def differentiate(step, carry):
        rows = full_g[pl.ds(step * 2, 2)].reshape(512, 2048)
        at = pl.ds(pl.multiple_of(step * 512, 512), 512)
        hidden_grad = dot_nt(rows, wd[...])
        up_grad[at, :] = (hidden_grad * silu_keep[at, :]).astype(BF)
        gate_grad[at, :] = (hidden_grad * slope_keep[at, :]).astype(BF)
        return carry

    lax.fori_loop(0, 2, differentiate, 0)
    save(full_g, g_hbm)
    save(gate_grad, gate_hbm)
    save(up_grad, up_hbm)
    for portion in portions:
        for copy in portion[0][:-1]:
            copy.wait_send()

    def partial_of(side, cut):
        at = pl.ds(pl.multiple_of(side * 1024 + cut[0], 128), cut[1])
        return dot_nt(gate_grad[...], wg[at, :]) + dot_nt(up_grad[...], wu[at, :])

    back_stages = (send.at[1], back.at[0], back.at[1], back.at[2])
    returns = [
        [
            phase_copies(
                (back_stages[phase], cut[0]),
                (back_stages[phase + 1], cut[0]),
                ORDERS[which][phase],
                cut[1],
                send_sems.at[6 + which, phase],
                recv_sems.at[6 + which, phase],
                local_sems.at[6 + which, phase],
            )
            for phase in range(3)
        ]
        for which, cut in enumerate(X_CUTS)
    ]
    shares = []
    for which, cut in enumerate(X_CUTS):
        columns = pl.ds(cut[0], cut[1])
        send[0, :, :, :, :, columns] = (
            partial_of(1 - tp, cut).astype(BF).reshape(4, 4, 4, SLOTS, cut[1])
        )
        share = remote(
            send.at[0, :, :, :, :, columns],
            arrived.at[:, :, :, :, columns],
            tp_send.at[6 + which],
            tp_recv.at[6 + which],
            partner,
        )
        share.start()
        shares.append(share)
    for which, cut in enumerate(X_CUTS):
        columns = pl.ds(cut[0], cut[1])
        mine = partial_of(tp, cut).astype(BF).astype(F32)
        shares[which].wait_recv()
        theirs = arrived[:, :, :, :, columns].reshape(1024, cut[1]).astype(F32)
        send[1, :, :, :, :, columns] = (mine + theirs).astype(BF).reshape(4, 4, 4, SLOTS, cut[1])
        start_all(returns[which][0])
    for phase in range(1, 3):
        for portion in returns:
            arrive_all(portion[phase - 1])
            start_all(portion[phase])

    swaps = []
    for which, portion in enumerate(returns):
        arrive_all(portion[2])
        cut = X_CUTS[which]
        columns = pl.ds(cut[0], cut[1])
        added = dot_tn(hot_ref[...], back[2, :, :, :, :, columns].reshape(1024, cut[1]))
        total = (cot_ref[:, columns].astype(F32) + added).astype(BF)
        half_ref[:, columns] = total
        whole[tp, :, columns] = total
        swap = remote(
            whole.at[tp, :, columns],
            whole.at[tp, :, columns],
            tp_send.at[9 + which],
            tp_recv.at[9 + which],
            partner,
        )
        swap.start()
        swaps.append(swap)

    def block_of(half):
        for part in range(2):
            product = dot_tn(whole[half, :, pl.ds(part * 512, 512)], mixer_out[...])
            for tile in range(4):
                blocks[half * 2 + part, :, :, pl.ds(tile * 2, 2)] = (
                    product[:, tile * 128 : (tile + 1) * 128].astype(BF).reshape(4, 4, 2, 16, 128)
                )

    block_of(tp)
    for swap in swaps:
        swap.wait()
    block_of(1 - tp)

    def fold_copies(which, phase):
        start, count = UNIT_CUTS[which]
        dim = ORDERS[which][phase]
        here = coordinate(dim)
        left_dims = sorted(ORDERS[which][phase:])
        copies = []
        for by in (2, 1, 3):
            index = [slice(None)] * len(left_dims)
            index[left_dims.index(dim)] = (here + by) % SIDE
            units = pl.ds(start, count)
            if phase == 0:
                source = blocks.at[(*index, units)]
                target = got1.at[by - 1, :, :, units]
            elif phase == 1:
                source = sum1.at[(*index, units)]
                target = got2.at[by - 1, :, units]
            else:
                source = sum2.at[(*index, units)]
                target = got3.at[by - 1, units]
            copies.append(
                remote(
                    source,
                    target,
                    fold_send.at[which, phase, by - 1],
                    fold_recv.at[which, phase, by - 1],
                    (peer_of(dim, by), tp),
                )
            )
        return copies

    def folded(which, phase):
        start, count = UNIT_CUTS[which]
        units = pl.ds(start, count)
        dim = ORDERS[which][phase]
        left_dims = sorted(ORDERS[which][phase:])
        index = [slice(None)] * len(left_dims)
        index[left_dims.index(dim)] = coordinate(dim)
        source = (blocks, sum1, sum2)[phase]
        total = source[(*index, units)].astype(F32)
        for by in range(3):
            if phase == 0:
                total = total + got1[by, :, :, units].astype(F32)
            elif phase == 1:
                total = total + got2[by, :, units].astype(F32)
            else:
                total = total + got3[by, units].astype(F32)
        return total

    folds = [[fold_copies(which, phase) for phase in range(3)] for which in range(3)]
    for fold in folds:
        start_all(fold[0])

    mixer_grad = (dot(whole[0], w_out[0:1024, :]) + dot(whole[1], w_out[1024:2048, :])).astype(BF)
    mixer_wide = mixer_grad.astype(F32)
    gate_in_grad_ref[...] = (mixer_wide * conv_sum_ref[...]).astype(BF)
    pad_right[pl.ds(0, 256), :] = mixer_wide * gate_in_ref[...].astype(F32)
    right = remote(
        pad_right.at[pl.ds(0, 8)],
        halo.at[1],
        halo_send.at[1],
        halo_recv.at[1],
        ((sp + 63) % 64, tp),
    )
    right.start()
    for which, fold in enumerate(folds):
        start, count = UNIT_CUTS[which]
        for copy in fold[0]:
            copy.wait_recv()
        sum1[:, :, pl.ds(start, count)] = folded(which, 0).astype(BF)
        start_all(fold[1])
    right.wait()
    pad_right[pl.ds(256, 8), :] = jnp.where(sp == 63, 0.0, halo[1])
    prod_grad = jnp.zeros((256, 512), F32)
    for tap in range(3):
        prod_grad = prod_grad + taps_ref[tap : tap + 1, :] * pad_right[pl.ds(2 - tap, 256), :]
    conv_gate_grad_ref[...] = (prod_grad * conv_value_ref[...].astype(F32)).astype(BF)
    conv_value_grad_ref[...] = (prod_grad * conv_gate_ref[...].astype(F32)).astype(BF)
    for which, fold in enumerate(folds):
        start, count = UNIT_CUTS[which]
        for copy in fold[1]:
            copy.wait_recv()
        sum2[:, pl.ds(start, count)] = folded(which, 1).astype(BF)
        start_all(fold[2])
    for which, fold in enumerate(folds):
        start, count = UNIT_CUTS[which]
        for copy in fold[2]:
            copy.wait_recv()
        total = folded(which, 2)
        for unit in range(count):
            tile, row = divmod(start + unit, 2)
            out_block_ref[pl.ds(row * 16, 16), pl.ds(tile * 128, 128)] = total[unit]
    for share in shares:
        share.wait_send()
    for portion in portions:
        for copies in portion[1:]:
            for copy in copies[:-1]:
                copy.wait_send()
    for portion in returns:
        for copies in portion:
            for copy in copies[:-1]:
                copy.wait_send()
    for fold in folds:
        for copies in fold:
            for copy in copies:
                copy.wait_send()
    for copy in saves:
        copy.wait()


def main_call(*operands):
    vmem = pl.BlockSpec(memory_space=pltpu.VMEM)
    hbm = pl.BlockSpec(memory_space=pl.ANY)
    shape = jax.ShapeDtypeStruct
    rows_shape = (4, 4, 4, SLOTS, 1024)
    full_shape = (4, 4, 4, SLOTS, 2048)
    dma = pltpu.SemaphoreType.DMA
    return pl.pallas_call(
        main_kernel,
        out_shape=(
            shape((256, 1024), BF),
            shape((256, 512), BF),
            shape((256, 512), BF),
            shape((256, 512), BF),
            shape((32, 512), F32),
            shape(full_shape, BF),
            shape(full_shape, BF),
            shape((1024, 512), BF),
            shape((1024, 512), BF),
            shape((1024, 512), BF),
        ),
        in_specs=[vmem] * 8 + [hbm] * 4,
        out_specs=(vmem,) * 5 + (hbm,) * 5,
        scratch_shapes=[
            pltpu.VMEM((2, *rows_shape), BF),
            pltpu.VMEM((2, 2, *rows_shape), BF),
            pltpu.VMEM(full_shape, BF),
            pltpu.VMEM(full_shape, BF),
            pltpu.VMEM((2048, 512), BF),
            pltpu.VMEM((2048, 512), BF),
            pltpu.VMEM((512, 2048), BF),
            pltpu.VMEM((2048, 512), BF),
            pltpu.VMEM((1024, 512), F32),
            pltpu.VMEM((1024, 512), F32),
            pltpu.VMEM((1024, 512), BF),
            pltpu.VMEM((1024, 512), BF),
            pltpu.VMEM((1024, 512), BF),
            pltpu.VMEM(rows_shape, BF),
            pltpu.VMEM((3, *rows_shape), BF),
            pltpu.VMEM((1024, 256), BF),
            pltpu.VMEM((2, 256, 1024), BF),
            pltpu.VMEM((4, 4, 4, 8, 16, 128), BF),
            pltpu.VMEM((3, 4, 4, 8, 16, 128), BF),
            pltpu.VMEM((4, 4, 8, 16, 128), BF),
            pltpu.VMEM((3, 4, 8, 16, 128), BF),
            pltpu.VMEM((4, 8, 16, 128), BF),
            pltpu.VMEM((3, 8, 16, 128), BF),
            pltpu.VMEM((264, 512), F32),
            pltpu.VMEM((264, 512), F32),
            pltpu.VMEM((2, 8, 512), F32),
            pltpu.VMEM((256, 512), F32),
            pltpu.VMEM((256, 512), BF),
            dma((4,)),
            dma((5,)),
            dma((9, 3, 3)),
            dma((9, 3, 3)),
            dma((9, 3)),
            dma((12,)),
            dma((12,)),
            dma((2,)),
            dma((2,)),
            dma((3, 3, 3)),
            dma((3, 3, 3)),
        ],
        compiler_params=pltpu.CompilerParams(
            collective_id=0, has_side_effects=True, vmem_limit_bytes=67043328
        ),
    )(*operands)


def shards(
    stream,
    out_grad,
    gate_in,
    conv_gate,
    conv_value,
    taps,
    w_out,
    route_ids,
    route_weights,
    w_gate,
    w_up,
    w_down,
):
    half, gate_in_grad, conv_gate_grad, conv_value_grad, out_block, x, g, hidden, gate, up = main_call(
        route_ids.T,
        route_weights.T,
        stream,
        out_grad,
        gate_in,
        conv_gate,
        conv_value,
        taps,
        w_out,
        w_gate,
        w_up,
        w_down,
    )
    x = x.reshape(1024, 2048)
    g = g.reshape(1024, 2048)
    return (
        half,
        gate_in_grad,
        conv_gate_grad,
        conv_value_grad,
        out_block,
        dot_tn(x, gate)[None],
        dot_tn(x, up)[None],
        dot_tn(hidden, g)[None],
    )


def solution(mesh):
    placed = (
        P("sp", "tp"),
        P("sp", "tp"),
        P("sp", "tp"),
        P("sp", "tp"),
        P("sp", "tp"),
        P(None, "tp"),
        P(None, "tp"),
        P("sp", None),
        P("sp", None),
        P("sp", None, "tp"),
        P("sp", None, "tp"),
        P("sp", "tp", None),
    )
    return jax.shard_map(
        shards,
        mesh=mesh,
        in_specs=placed,
        out_specs=(
            P("sp", "tp"),
            P("sp", "tp"),
            P("sp", "tp"),
            P("sp", "tp"),
            P("sp", "tp"),
            P("sp", None, "tp"),
            P("sp", None, "tp"),
            P("sp", "tp", None),
        ),
        check_vma=False,
    )
```

profile of v0, /device:TPU:0, one launch (start us, length us, event | category | flops | bytes accessed | tf_op | source)
XLA Modules:
  0.0 152.6 jit_solution(15204037645877587591)
XLA Ops:
  0.6 132.4 %shard_map.179 = (bf16[256,1024]{1,0:T(8,128)(2,1)}, bf16[256,512]{1,0:T(8,128)(2,1)}, bf16[256,512]{1,0:T(8,128)(2,1)}, bf16[256,512]{1,0:T(8,128)(2,1)}, f32[3...) custom-call(s32[2,256]{1,0:T(2,128)} %bitcast.17, ...), custom_call_target="tpu_custom_call" | custom-call | tf_op jit(solution)/shard_map/pallas_call | solution.py:536
  133.0 0.0 copy-start.7
  133.0 0.0 copy-start.8
  133.1 7.0 %convolution_bitcast_fusion.1 = f32[1,2048,512]{2,1,0:T(8,128)} fusion(bf16[1024,2048]{1,0:T(8,128)(2,1)} %bitcast.19, bf16[1024,512]{1,0:T(8,128)(2,1)} %get-tuple-element.25), kind=kOutput, calls=%fused_computation.1 | convolution fusion | flops 2147483648 | bytes 9437184 | tf_op jit(solution)/shard_map/dot_general | solution.py:126
  140.1 0.0 copy-done.7
  140.1 0.0 copy-done.8
  140.1 0.0 copy-start
  140.1 0.0 copy-start.1
  140.1 4.5 %convolution_bitcast_fusion.2 = f32[1,2048,512]{2,1,0:T(8,128)} fusion(bf16[1024,2048]{1,0:T(8,128)(2,1)S(1)} %bitcast.20, bf16[1024,512]{1,0:T(8,128)(2,1)S(1)} %copy-done.8), kind=kOutput, calls=%fused_computation.2 | convolution fusion | flops 2147483648 | bytes 9437184 | tf_op jit(solution)/shard_map/dot_general | solution.py:126
  144.6 0.0 copy-done
  144.6 0.0 copy-done.1
  144.6 0.0 copy-start.2
  144.6 0.0 copy-start.5
  144.6 0.0 copy-start.4
  144.6 0.0 copy-start.3
  144.6 0.0 copy-start.6
  144.6 4.4 %convolution_bitcast_fusion = f32[1,512,2048]{2,1,0:T(8,128)} fusion(bf16[1024,512]{1,0:T(8,128)(2,1)S(1)} %copy-done.1, bf16[1024,2048]{1,0:T(8,128)(2,1)S(1)} %bitcast.16), kind=kOutput, calls=%fused_computation | convolution fusion | flops 2147483648 | bytes 9437184 | tf_op jit(solution)/shard_map/dot_general | solution.py:126
  149.1 0.0 copy-done.2
  149.1 0.8 copy.25
  149.8 0.0 copy-done.5
  149.8 0.7 copy.26
  150.6 0.0 copy-done.4
  150.6 0.7 copy.27
  151.3 0.0 copy-done.3
  151.3 0.7 copy.28
  152.0 0.0 copy-done.6
  152.0 0.6 copy.29
Async XLA Ops:
  133.0 7.1 %copy-start.7 = (bf16[4,4,4,16,2048]{4,3,2,1,0:T(8,128)(2,1)S(1)}, bf16[4,4,4,16,2048]{4,3,2,1,0:T(8,128)(2,1)}, u32[]{:S(2)}) copy-start(bf16[4,4,4,16,2048]{4,3,2,1,0:T(8,128)(2,1)} %get-tuple-element.23) | copy-start | bytes 12582916
  133.0 7.0 %copy-start.8 = (bf16[1024,512]{1,0:T(8,128)(2,1)S(1)}, bf16[1024,512]{1,0:T(8,128)(2,1)}, u32[]{:S(2)}) copy-start(bf16[1024,512]{1,0:T(8,128)(2,1)} %get-tuple-element.24) | copy-start | bytes 3145732
  140.1 4.5 %copy-start = (bf16[4,4,4,16,2048]{4,3,2,1,0:T(8,128)(2,1)S(1)}, bf16[4,4,4,16,2048]{4,3,2,1,0:T(8,128)(2,1)}, u32[]{:S(2)}) copy-start(bf16[4,4,4,16,2048]{4,3,2,1,0:T(8,128)(2,1)} %get-tuple-element.27) | copy-start | bytes 12582916
  140.1 4.5 %copy-start.1 = (bf16[1024,512]{1,0:T(8,128)(2,1)S(1)}, bf16[1024,512]{1,0:T(8,128)(2,1)}, u32[]{:S(2)}) copy-start(bf16[1024,512]{1,0:T(8,128)(2,1)} %get-tuple-element.26) | copy-start | bytes 3145732
  144.6 4.5 %copy-start.2 = (bf16[256,1024]{1,0:T(8,128)(2,1)S(1)}, bf16[256,1024]{1,0:T(8,128)(2,1)}, u32[]{:S(2)}) copy-start(bf16[256,1024]{1,0:T(8,128)(2,1)} %get-tuple-element.36) | copy-start | bytes 1572868
  144.6 5.3 %copy-start.5 = (bf16[256,512]{1,0:T(8,128)(2,1)S(1)}, bf16[256,512]{1,0:T(8,128)(2,1)}, u32[]{:S(2)}) copy-start(bf16[256,512]{1,0:T(8,128)(2,1)} %get-tuple-element.37) | copy-start | bytes 786436
  144.6 6.0 %copy-start.4 = (bf16[256,512]{1,0:T(8,128)(2,1)S(1)}, bf16[256,512]{1,0:T(8,128)(2,1)}, u32[]{:S(2)}) copy-start(bf16[256,512]{1,0:T(8,128)(2,1)} %get-tuple-element.38) | copy-start | bytes 786436
  144.6 6.7 %copy-start.3 = (bf16[256,512]{1,0:T(8,128)(2,1)S(1)}, bf16[256,512]{1,0:T(8,128)(2,1)}, u32[]{:S(2)}) copy-start(bf16[256,512]{1,0:T(8,128)(2,1)} %get-tuple-element.39) | copy-start | bytes 786436
  144.6 7.4 %copy-start.6 = (f32[32,512]{1,0:T(8,128)S(1)}, f32[32,512]{1,0:T(8,128)}, u32[]{:S(2)}) copy-start(f32[32,512]{1,0:T(8,128)} %get-tuple-element.40) | copy-start | bytes 196612
where the time goes:
time: 153 us
  Pallas kernels  132 us (86%)
  matrix products  15.9 us (10%)
  local copies, waits for them, and re-layouts  3.57 us (2%)
    pallas_call x1, Pallas kernels, main_call(): pl.pallas_call(main_kernel, out_shape=(shape((256, 1024), BF), shape((256...  132 us
    dot_general x3, matrix products, dot_tn(): lax.dot_general(a, b, (((0,), (0,)), ((), ())), preferred_element_type=F32)  15.9 us
    unnamed x23, local copies, waits for them, and re-layouts  3.57 us

commit v1 on v0

--- a/solution.py
+++ b/solution.py
@@ -14,8 +14,13 @@
 SLOTS = 16
 STRIDE = (16, 4, 1)
 ORDERS = ((2, 1, 0), (1, 0, 2), (0, 2, 1))
-X_CUTS = ((0, 384), (384, 384), (768, 256))
-G_CUTS = ((0, 256), (256, 384), (640, 384))
+Z_OFFSETS = (0, 2, 1, 3)
+LATE_SHORT = ((0, 384), (384, 384), (768, 256))
+EARLY_SHORT = ((0, 256), (256, 384), (640, 384))
+MIDDLE_SHORT = ((0, 384), (384, 256), (640, 384))
+X_CUTS = (LATE_SHORT, MIDDLE_SHORT)
+G_CUTS = (EARLY_SHORT, LATE_SHORT)
+BACK_CUTS = (MIDDLE_SHORT, EARLY_SHORT)
 
 
 def coordinate(dim):
@@ -27,45 +32,75 @@
     return lax.axis_index("sp") + ((here + by) % SIDE - here) * STRIDE[dim]
 
 
-def piece(spot, dim, at, width):
+def piece(spot, index, width):
     ref, start = spot
-    index = [slice(None)] * 3
-    index[dim] = at
     return ref.at[(*index, slice(None), pl.ds(start, width))]
 
 
-def phase_copies(source, target, dim, width, send_sem, recv_sem, local_sem):
+def phase_copies(source, target, dim, width, chunk, send_sem, recv_sem, local_sem):
     here = coordinate(dim)
     tp = lax.axis_index("tp")
-    copies = []
-    for by in (2, 1, 3):
-        copies.append(
-            pltpu.make_async_remote_copy(
-                src_ref=piece(source, dim, (here + by) % SIDE, width),
-                dst_ref=piece(target, dim, here, width),
-                send_sem=send_sem.at[by - 1],
-                recv_sem=recv_sem.at[by - 1],
-                device_id=(peer_of(dim, by), tp),
-                device_id_type=MESH,
+    moves = []
+    if dim == 0:
+        every = (slice(None), slice(None))
+        if chunk == 0:
+            kept = ((0, *every), (0, *every))
+            moves.append((2, (1, *every), (1, *every)))
+        else:
+            kept = None
+            moves.append((1, (2, *every), (3, *every)))
+            moves.append((3, (3, *every), (2, *every)))
+    else:
+
+        def at(place):
+            index = [pl.ds(2 * chunk, 2), slice(None), slice(None)]
+            index[dim] = place
+            return tuple(index)
+
+        kept = (at(here), at(here))
+        for by in (2, 1, 3):
+            moves.append((by, at((here + by) % SIDE), at(here)))
+    sent = [
+        pltpu.make_async_remote_copy(
+            src_ref=piece(source, from_index, width),
+            dst_ref=piece(target, to_index, width),
+            send_sem=send_sem.at[by - 1],
+            recv_sem=recv_sem.at[by - 1],
+            device_id=(peer_of(dim, by), tp),
+            device_id_type=MESH,
+        )
+        for by, from_index, to_index in moves
+    ]
+    local = []
+    if kept is not None:
+        local.append(
+            pltpu.make_async_copy(
+                piece(source, kept[0], width), piece(target, kept[1], width), local_sem
             )
         )
-    copies.append(
-        pltpu.make_async_copy(
-            piece(source, dim, here, width), piece(target, dim, here, width), local_sem
-        )
-    )
-    return copies
+    return sent, local
+
+
+def start_phase(copies):
+    for copy in copies[0] + copies[1]:
+        copy.start()
+
+
+def arrive_phase(copies):
+    for copy in copies[0]:
+        copy.wait_recv()
+    for copy in copies[1]:
+        copy.wait()
+
+
+def sent_phase(copies):
+    for copy in copies[0]:
+        copy.wait_send()
 
 
 def start_all(copies):
     for copy in copies:
         copy.start()
-
-
-def arrive_all(copies):
-    for copy in copies[:-1]:
-        copy.wait_recv()
-    copies[-1].wait()
 
 
 def slots_in_lanes(ids):
@@ -166,8 +201,11 @@
     hidden,
     gate_grad,
     up_grad,
+    shared,
     arrived,
+    rows_out,
     back,
+    added_ref,
     hot_ref,
     whole,
     blocks,
@@ -207,27 +245,37 @@
 
     slot0, slot1 = slots_in_lanes(ids_ref[...])
     weight0, weight1 = weights_ref[0:1, :], weights_ref[1:2, :]
-    for z in range(SIDE):
-        row = lax.broadcasted_iota(jnp.int32, (256, 256), 0) + z * 256
-        hot = jnp.where((row == slot0) | (row == slot1), 1.0, 0.0).astype(BF)
-        hot_ref[pl.ds(z * 256, 256), :] = hot
-        send[0, z] = dot(hot, stream_ref[...]).astype(BF).reshape(4, 4, SLOTS, 1024)
-
-    def own_half(ref, cut):
-        start = pl.multiple_of(tp * 1024 + cut[0], 128)
-        return ref.at[:, :, :, :, pl.ds(start, cut[1])]
+
+    def row_numbers(place):
+        z = (coordinate(0) + Z_OFFSETS[place]) % SIDE
+        return lax.broadcasted_iota(jnp.int32, (256, 256), 0) + z * 256
+
+    def gather_x(chunk):
+        for place in (2 * chunk, 2 * chunk + 1):
+            row = row_numbers(place)
+            hot = jnp.where((row == slot0) | (row == slot1), 1.0, 0.0).astype(BF)
+            hot_ref[pl.ds(place * 256, 256), :] = hot
+            send[0, place] = dot(hot, stream_ref[...]).astype(BF).reshape(4, 4, SLOTS, 1024)
+
+    def gather_g(chunk):
+        for place in (2 * chunk, 2 * chunk + 1):
+            row = row_numbers(place)
+            scale = jnp.sum(
+                jnp.where(row == slot0, weight0, 0.0) + jnp.where(row == slot1, weight1, 0.0),
+                axis=1,
+                keepdims=True,
+            )
+            hot = hot_ref[pl.ds(place * 256, 256), :]
+            send[1, place] = (
+                (scale * dot(hot, cot_ref[...])).astype(BF).reshape(4, 4, SLOTS, 1024)
+            )
 
     full = (full_x, full_g)
-    portions = []
-    for tensor, cuts in enumerate((X_CUTS, G_CUTS)):
+
+    def stream_of(number, spots_of, cuts, chunk):
+        portions = []
         for which, cut in enumerate(cuts):
-            number = tensor * 3 + which
-            spots = [
-                (send.at[tensor], cut[0]),
-                (middle.at[0, tensor], cut[0]),
-                (middle.at[1, tensor], cut[0]),
-                (full[tensor], pl.multiple_of(tp * 1024 + cut[0], 128)),
-            ]
+            spots = spots_of(cut)
             portions.append(
                 [
                     phase_copies(
@@ -235,28 +283,142 @@
                         spots[phase + 1],
                         ORDERS[which][phase],
                         cut[1],
-                        send_sems.at[number, phase],
-                        recv_sems.at[number, phase],
-                        local_sems.at[number, phase],
+                        chunk,
+                        send_sems.at[number * 3 + which, phase],
+                        recv_sems.at[number * 3 + which, phase],
+                        local_sems.at[number * 3 + which, phase],
                     )
                     for phase in range(3)
                 ]
             )
+        return portions
+
+    def outward(tensor, chunk):
+        return stream_of(
+            chunk * 2 + tensor,
+            lambda cut: (
+                (send.at[tensor], cut[0]),
+                (middle.at[0, tensor], cut[0]),
+                (middle.at[1, tensor], cut[0]),
+                (full[tensor], pl.multiple_of(tp * 1024 + cut[0], 128)),
+            ),
+            (X_CUTS, G_CUTS)[tensor][chunk],
+            chunk,
+        )
+
+    def homeward(chunk):
+        return stream_of(
+            4 + chunk,
+            lambda cut: (
+                (rows_out, cut[0]),
+                (back.at[0], cut[0]),
+                (back.at[1], cut[0]),
+                (back.at[2], cut[0]),
+            ),
+            BACK_CUTS[chunk],
+            chunk,
+        )
+
+    xs = [outward(0, chunk) for chunk in range(2)]
+    gs = [outward(1, chunk) for chunk in range(2)]
+    backs = [homeward(chunk) for chunk in range(2)]
+
+    def begin(portions):
+        for portion in portions:
+            start_phase(portion[0])
+
+    def advance(portions, phase):
+        for portion in portions:
+            arrive_phase(portion[phase - 1])
+            start_phase(portion[phase])
+
+    crossings = {}
+    saves = []
+
+    def cross(tensor, chunk):
+        crossings[tensor, chunk] = []
+        portions = (xs, gs)[tensor][chunk]
+        for which, cut in enumerate((X_CUTS, G_CUTS)[tensor][chunk]):
+            number = (chunk * 2 + tensor) * 3 + which
+            arrive_phase(portions[which][2])
+            start = pl.multiple_of(tp * 1024 + cut[0], 128)
+            part = full[tensor].at[pl.ds(2 * chunk, 2), :, :, :, pl.ds(start, cut[1])]
+            crossing = remote(part, part, tp_send.at[number], tp_recv.at[number], partner)
+            crossing.start()
+            crossings[tensor, chunk].append(crossing)
+
+    def crossed(tensor, chunk):
+        for crossing in crossings[tensor, chunk]:
+            crossing.wait()
+
+    def save(source, target):
+        copy = pltpu.make_async_copy(source, target, save_sems.at[len(saves)])
+        copy.start()
+        saves.append(copy)
+
+    def activate(chunk):
+        rows = full_x[pl.ds(chunk * 2, 2)].reshape(512, 2048)
+        at = pl.ds(chunk * 512, 512)
+        pre_gate = dot(rows, wg[...])
+        pre_up = dot(rows, wu[...])
+        sigmoid = jax.nn.sigmoid(pre_gate)
+        silu = pre_gate * sigmoid
+        silu_keep[at, :] = silu
+        slope_keep[at, :] = pre_up * sigmoid * (1.0 + pre_gate * (1.0 - sigmoid))
+        hidden[at, :] = (silu * pre_up).astype(BF)
+
+    def differentiate(chunk):
+        rows = full_g[pl.ds(chunk * 2, 2)].reshape(512, 2048)
+        at = pl.ds(chunk * 512, 512)
+        hidden_grad = dot_nt(rows, wd[...])
+        up_grad[at, :] = (hidden_grad * silu_keep[at, :]).astype(BF)
+        gate_grad[at, :] = (hidden_grad * slope_keep[at, :]).astype(BF)
+
+    def partial_of(side, cut, chunk):
+        at = pl.ds(pl.multiple_of(side * 1024 + cut[0], 128), cut[1])
+        rows = pl.ds(chunk * 512, 512)
+        return dot_nt(gate_grad[rows, :], wg[at, :]) + dot_nt(up_grad[rows, :], wu[at, :])
+
+    shares = {}
+
+    def part(chunk, cut):
+        return (pl.ds(2 * chunk, 2), slice(None), slice(None), slice(None), pl.ds(*cut))
+
+    def share_theirs(chunk):
+        shares[chunk] = []
+        for which, cut in enumerate(BACK_CUTS[chunk]):
+            index = part(chunk, cut)
+            shared[index] = (
+                partial_of(1 - tp, cut, chunk).astype(BF).reshape(2, 4, 4, SLOTS, cut[1])
+            )
+            number = 12 + chunk * 3 + which
+            share = remote(
+                shared.at[index],
+                arrived.at[index],
+                tp_send.at[number],
+                tp_recv.at[number],
+                partner,
+            )
+            share.start()
+            shares[chunk].append(share)
+
+    def add_mine(chunk, begin_return):
+        for which, cut in enumerate(BACK_CUTS[chunk]):
+            index = part(chunk, cut)
+            mine = partial_of(tp, cut, chunk).astype(BF).astype(F32)
+            shares[chunk][which].wait_recv()
+            theirs = arrived[index].reshape(512, cut[1]).astype(F32)
+            rows_out[index] = (mine + theirs).astype(BF).reshape(2, 4, 4, SLOTS, cut[1])
+            if begin_return:
+                start_phase(backs[chunk][which][0])
+
+    gather_x(0)
     all_greeted()
-    for portion in portions[:3]:
-        start_all(portion[0])
-    for z in range(SIDE):
-        row = lax.broadcasted_iota(jnp.int32, (256, 256), 0) + z * 256
-        scale = jnp.sum(
-            jnp.where(row == slot0, weight0, 0.0) + jnp.where(row == slot1, weight1, 0.0),
-            axis=1,
-            keepdims=True,
-        )
-        hot = hot_ref[pl.ds(z * 256, 256), :]
-        send[1, z] = (scale * dot(hot, cot_ref[...])).astype(BF).reshape(4, 4, SLOTS, 1024)
-    for portion in portions[3:]:
-        start_all(portion[0])
-
+    begin(xs[0])
+    gather_g(0)
+    begin(gs[0])
+    gather_x(1)
+    gather_g(1)
     pad_left[pl.ds(8, 256), :] = conv_gate_ref[...].astype(F32) * conv_value_ref[...].astype(F32)
     left = remote(
         pad_left.at[pl.ds(256, 8)],
@@ -266,9 +428,8 @@
         ((sp + 1) % 64, tp),
     )
     left.start()
-    for portion in portions:
-        arrive_all(portion[0])
-        start_all(portion[1])
+    advance(xs[0], 1)
+    advance(gs[0], 1)
     left.wait()
     pad_left[pl.ds(0, 8), :] = jnp.where(sp == 0, 0.0, halo[0])
     conv_sum = jnp.zeros((256, 512), F32)
@@ -276,129 +437,62 @@
         conv_sum = conv_sum + taps_ref[tap : tap + 1, :] * pad_left[pl.ds(6 + tap, 256), :]
     conv_sum_ref[...] = conv_sum
     mixer_out[...] = (gate_in_ref[...].astype(F32) * conv_sum).astype(BF)
-    for portion in portions:
-        arrive_all(portion[1])
-        start_all(portion[2])
-
-    crossings = []
-    saves = []
-
-    def cross(tensor):
-        for which, cut in enumerate((X_CUTS, G_CUTS)[tensor]):
-            number = tensor * 3 + which
-            arrive_all(portions[number][2])
-            part = own_half(full[tensor], cut)
-            crossing = remote(part, part, tp_send.at[number], tp_recv.at[number], partner)
-            crossing.start()
-            crossings.append(crossing)
-
-    def save(source, target):
-        copy = pltpu.make_async_copy(source, target, save_sems.at[len(saves)])
-        copy.start()
-        saves.append(copy)
-
-    cross(0)
+    advance(xs[0], 2)
+    advance(gs[0], 2)
+    begin(xs[1])
+    cross(0, 0)
+    begin(gs[1])
+    cross(1, 0)
     for load in loads:
         load.wait()
-    for crossing in crossings[:3]:
-        crossing.wait()
-
-    def activate(step, carry):
-        rows = full_x[pl.ds(step * 2, 2)].reshape(512, 2048)
-        at = pl.ds(pl.multiple_of(step * 512, 512), 512)
-        pre_gate = dot(rows, wg[...])
-        pre_up = dot(rows, wu[...])
-        sigmoid = jax.nn.sigmoid(pre_gate)
-        silu = pre_gate * sigmoid
-        silu_keep[at, :] = silu
-        slope_keep[at, :] = pre_up * sigmoid * (1.0 + pre_gate * (1.0 - sigmoid))
-        hidden[at, :] = (silu * pre_up).astype(BF)
-        return carry
-
-    lax.fori_loop(0, 2, activate, 0)
+    crossed(0, 0)
+    activate(0)
+    advance(xs[1], 1)
+    crossed(1, 0)
+    differentiate(0)
+    advance(gs[1], 1)
+    share_theirs(0)
+    advance(xs[1], 2)
+    add_mine(0, False)
+    advance(gs[1], 2)
+    begin(backs[0])
+    cross(0, 1)
+    crossed(0, 1)
+    activate(1)
     save(full_x, x_hbm)
     save(hidden, hidden_hbm)
-    cross(1)
-    for crossing in crossings[3:]:
-        crossing.wait()
-
-    def differentiate(step, carry):
-        rows = full_g[pl.ds(step * 2, 2)].reshape(512, 2048)
-        at = pl.ds(pl.multiple_of(step * 512, 512), 512)
-        hidden_grad = dot_nt(rows, wd[...])
-        up_grad[at, :] = (hidden_grad * silu_keep[at, :]).astype(BF)
-        gate_grad[at, :] = (hidden_grad * slope_keep[at, :]).astype(BF)
-        return carry
-
-    lax.fori_loop(0, 2, differentiate, 0)
+    advance(backs[0], 1)
+    cross(1, 1)
+    crossed(1, 1)
+    differentiate(1)
     save(full_g, g_hbm)
     save(gate_grad, gate_hbm)
     save(up_grad, up_hbm)
-    for portion in portions:
-        for copy in portion[0][:-1]:
-            copy.wait_send()
-
-    def partial_of(side, cut):
-        at = pl.ds(pl.multiple_of(side * 1024 + cut[0], 128), cut[1])
-        return dot_nt(gate_grad[...], wg[at, :]) + dot_nt(up_grad[...], wu[at, :])
-
-    back_stages = (send.at[1], back.at[0], back.at[1], back.at[2])
-    returns = [
-        [
-            phase_copies(
-                (back_stages[phase], cut[0]),
-                (back_stages[phase + 1], cut[0]),
-                ORDERS[which][phase],
-                cut[1],
-                send_sems.at[6 + which, phase],
-                recv_sems.at[6 + which, phase],
-                local_sems.at[6 + which, phase],
-            )
-            for phase in range(3)
-        ]
-        for which, cut in enumerate(X_CUTS)
-    ]
-    shares = []
-    for which, cut in enumerate(X_CUTS):
-        columns = pl.ds(cut[0], cut[1])
-        send[0, :, :, :, :, columns] = (
-            partial_of(1 - tp, cut).astype(BF).reshape(4, 4, 4, SLOTS, cut[1])
-        )
-        share = remote(
-            send.at[0, :, :, :, :, columns],
-            arrived.at[:, :, :, :, columns],
-            tp_send.at[6 + which],
-            tp_recv.at[6 + which],
-            partner,
-        )
-        share.start()
-        shares.append(share)
-    for which, cut in enumerate(X_CUTS):
-        columns = pl.ds(cut[0], cut[1])
-        mine = partial_of(tp, cut).astype(BF).astype(F32)
-        shares[which].wait_recv()
-        theirs = arrived[:, :, :, :, columns].reshape(1024, cut[1]).astype(F32)
-        send[1, :, :, :, :, columns] = (mine + theirs).astype(BF).reshape(4, 4, 4, SLOTS, cut[1])
-        start_all(returns[which][0])
-    for phase in range(1, 3):
-        for portion in returns:
-            arrive_all(portion[phase - 1])
-            start_all(portion[phase])
+    share_theirs(1)
+    advance(backs[0], 2)
+    add_mine(1, True)
+    for portion in backs[0]:
+        arrive_phase(portion[2])
+    added_ref[...] = dot_tn(
+        hot_ref[pl.ds(0, 512), :], back[2, pl.ds(0, 2)].reshape(512, 1024)
+    ) + cot_ref[...].astype(F32)
+    advance(backs[1], 1)
+    advance(backs[1], 2)
 
     swaps = []
-    for which, portion in enumerate(returns):
-        arrive_all(portion[2])
-        cut = X_CUTS[which]
-        columns = pl.ds(cut[0], cut[1])
-        added = dot_tn(hot_ref[...], back[2, :, :, :, :, columns].reshape(1024, cut[1]))
-        total = (cot_ref[:, columns].astype(F32) + added).astype(BF)
+    for which, portion in enumerate(backs[1]):
+        arrive_phase(portion[2])
+        cut = BACK_CUTS[1][which]
+        columns = pl.ds(*cut)
+        rows = back[2, pl.ds(2, 2), :, :, :, columns].reshape(512, cut[1])
+        total = (added_ref[:, columns] + dot_tn(hot_ref[pl.ds(512, 512), :], rows)).astype(BF)
         half_ref[:, columns] = total
         whole[tp, :, columns] = total
         swap = remote(
             whole.at[tp, :, columns],
             whole.at[tp, :, columns],
-            tp_send.at[9 + which],
-            tp_recv.at[9 + which],
+            tp_send.at[18 + which],
+            tp_recv.at[18 + which],
             partner,
         )
         swap.start()
@@ -508,16 +602,13 @@
         for unit in range(count):
             tile, row = divmod(start + unit, 2)
             out_block_ref[pl.ds(row * 16, 16), pl.ds(tile * 128, 128)] = total[unit]
-    for share in shares:
-        share.wait_send()
-    for portion in portions:
-        for copies in portion[1:]:
-            for copy in copies[:-1]:
-                copy.wait_send()
-    for portion in returns:
-        for copies in portion:
-            for copy in copies[:-1]:
-                copy.wait_send()
+    for chunk in range(2):
+        for share in shares[chunk]:
+            share.wait_send()
+        for stream in (xs[chunk], gs[chunk], backs[chunk]):
+            for portion in stream:
+                for copies in portion:
+                    sent_phase(copies)
     for fold in folds:
         for copies in fold:
             for copy in copies:
@@ -564,7 +655,10 @@
             pltpu.VMEM((1024, 512), BF),
             pltpu.VMEM((1024, 512), BF),
             pltpu.VMEM(rows_shape, BF),
+            pltpu.VMEM(rows_shape, BF),
+            pltpu.VMEM(rows_shape, BF),
             pltpu.VMEM((3, *rows_shape), BF),
+            pltpu.VMEM((256, 1024), F32),
             pltpu.VMEM((1024, 256), BF),
             pltpu.VMEM((2, 256, 1024), BF),
             pltpu.VMEM((4, 4, 4, 8, 16, 128), BF),
@@ -580,11 +674,11 @@
             pltpu.VMEM((256, 512), BF),
             dma((4,)),
             dma((5,)),
-            dma((9, 3, 3)),
-            dma((9, 3, 3)),
-            dma((9, 3)),
-            dma((12,)),
-            dma((12,)),
+            dma((18, 3, 3)),
+            dma((18, 3, 3)),
+            dma((18, 3)),
+            dma((21,)),
+            dma((21,)),
             dma((2,)),
             dma((2,)),
             dma((3, 3, 3)),

time: 153 us -> 141 us (0.922)
  Pallas kernels: 132 us -> 121 us
    pallas_call x1, Pallas kernels: 132 us -> 121 us  [main_call(): pl.pallas_call(main_kernel, out_shape=(shape((256, 1024), BF), shape((256...]
where the time goes in v1:
time: 141 us
  Pallas kernels  121 us (86%)
  matrix products  15.9 us (11%)
  local copies, waits for them, and re-layouts  3.57 us (3%)
    pallas_call x1, Pallas kernels, main_call(): pl.pallas_call(main_kernel, out_shape=(shape((256, 1024), BF), shape((256...  121 us
    dot_general x3, matrix products, dot_tn(): lax.dot_general(a, b, (((0,), (0,)), ((), ())), preferred_element_type=F32)  15.9 us
    unnamed x23, local copies, waits for them, and re-layouts  3.57 us

profile of v1, /device:TPU:0, one launch (start us, length us, event | category | flops | bytes accessed | tf_op | source)
XLA Modules:
  0.0 140.8 jit_solution(16924779703055096309)
XLA Ops:
  0.6 120.6 %shard_map.179 = (bf16[256,1024]{1,0:T(8,128)(2,1)}, bf16[256,512]{1,0:T(8,128)(2,1)}, bf16[256,512]{1,0:T(8,128)(2,1)}, bf16[256,512]{1,0:T(8,128)(2,1)}, f32[3...) custom-call(s32[2,256]{1,0:T(2,128)} %bitcast.17, ...), custom_call_target="tpu_custom_call" | custom-call | tf_op jit(solution)/shard_map/pallas_call | solution.py:627
  121.2 0.0 copy-start.7
  121.3 0.0 copy-start.8
  121.3 7.0 %convolution_bitcast_fusion.1 = f32[1,2048,512]{2,1,0:T(8,128)} fusion(bf16[1024,2048]{1,0:T(8,128)(2,1)} %bitcast.19, bf16[1024,512]{1,0:T(8,128)(2,1)} %get-tuple-element.25), kind=kOutput, calls=%fused_computation.1 | convolution fusion | flops 2147483648 | bytes 9437184 | tf_op jit(solution)/shard_map/dot_general | solution.py:161
  128.3 0.0 copy-done.7
  128.3 0.0 copy-done.8
  128.3 0.0 copy-start
  128.3 0.0 copy-start.1
  128.3 4.5 %convolution_bitcast_fusion.2 = f32[1,2048,512]{2,1,0:T(8,128)} fusion(bf16[1024,2048]{1,0:T(8,128)(2,1)S(1)} %bitcast.20, bf16[1024,512]{1,0:T(8,128)(2,1)S(1)} %copy-done.8), kind=kOutput, calls=%fused_computation.2 | convolution fusion | flops 2147483648 | bytes 9437184 | tf_op jit(solution)/shard_map/dot_general | solution.py:161
  132.8 0.0 copy-done
  132.8 0.0 copy-done.1
  132.8 0.0 copy-start.2
  132.8 0.0 copy-start.5
  132.8 0.0 copy-start.4
  132.8 0.0 copy-start.3
  132.8 0.0 copy-start.6
  132.8 4.4 %convolution_bitcast_fusion = f32[1,512,2048]{2,1,0:T(8,128)} fusion(bf16[1024,512]{1,0:T(8,128)(2,1)S(1)} %copy-done.1, bf16[1024,2048]{1,0:T(8,128)(2,1)S(1)} %bitcast.16), kind=kOutput, calls=%fused_computation | convolution fusion | flops 2147483648 | bytes 9437184 | tf_op jit(solution)/shard_map/dot_general | solution.py:161
  137.3 0.0 copy-done.2
  137.3 0.8 copy.25
  138.1 0.0 copy-done.5
  138.1 0.7 copy.26
  138.8 0.0 copy-done.4
  138.8 0.7 copy.27
  139.5 0.0 copy-done.3
  139.5 0.7 copy.28
  140.2 0.0 copy-done.6
  140.2 0.6 copy.29
Async XLA Ops:
  121.2 7.1 %copy-start.7 = (bf16[4,4,4,16,2048]{4,3,2,1,0:T(8,128)(2,1)S(1)}, bf16[4,4,4,16,2048]{4,3,2,1,0:T(8,128)(2,1)}, u32[]{:S(2)}) copy-start(bf16[4,4,4,16,2048]{4,3,2,1,0:T(8,128)(2,1)} %get-tuple-element.23) | copy-start | bytes 12582916
  121.3 7.0 %copy-start.8 = (bf16[1024,512]{1,0:T(8,128)(2,1)S(1)}, bf16[1024,512]{1,0:T(8,128)(2,1)}, u32[]{:S(2)}) copy-start(bf16[1024,512]{1,0:T(8,128)(2,1)} %get-tuple-element.24) | copy-start | bytes 3145732
  128.3 4.5 %copy-start = (bf16[4,4,4,16,2048]{4,3,2,1,0:T(8,128)(2,1)S(1)}, bf16[4,4,4,16,2048]{4,3,2,1,0:T(8,128)(2,1)}, u32[]{:S(2)}) copy-start(bf16[4,4,4,16,2048]{4,3,2,1,0:T(8,128)(2,1)} %get-tuple-element.27) | copy-start | bytes 12582916
  128.3 4.5 %copy-start.1 = (bf16[1024,512]{1,0:T(8,128)(2,1)S(1)}, bf16[1024,512]{1,0:T(8,128)(2,1)}, u32[]{:S(2)}) copy-start(bf16[1024,512]{1,0:T(8,128)(2,1)} %get-tuple-element.26) | copy-start | bytes 3145732
  132.8 4.5 %copy-start.2 = (bf16[256,1024]{1,0:T(8,128)(2,1)S(1)}, bf16[256,1024]{1,0:T(8,128)(2,1)}, u32[]{:S(2)}) copy-start(bf16[256,1024]{1,0:T(8,128)(2,1)} %get-tuple-element.36) | copy-start | bytes 1572868
  132.8 5.3 %copy-start.5 = (bf16[256,512]{1,0:T(8,128)(2,1)S(1)}, bf16[256,512]{1,0:T(8,128)(2,1)}, u32[]{:S(2)}) copy-start(bf16[256,512]{1,0:T(8,128)(2,1)} %get-tuple-element.37) | copy-start | bytes 786436
  132.8 6.0 %copy-start.4 = (bf16[256,512]{1,0:T(8,128)(2,1)S(1)}, bf16[256,512]{1,0:T(8,128)(2,1)}, u32[]{:S(2)}) copy-start(bf16[256,512]{1,0:T(8,128)(2,1)} %get-tuple-element.38) | copy-start | bytes 786436
  132.8 6.7 %copy-start.3 = (bf16[256,512]{1,0:T(8,128)(2,1)S(1)}, bf16[256,512]{1,0:T(8,128)(2,1)}, u32[]{:S(2)}) copy-start(bf16[256,512]{1,0:T(8,128)(2,1)} %get-tuple-element.39) | copy-start | bytes 786436
  132.8 7.4 %copy-start.6 = (f32[32,512]{1,0:T(8,128)S(1)}, f32[32,512]{1,0:T(8,128)}, u32[]{:S(2)}) copy-start(f32[32,512]{1,0:T(8,128)} %get-tuple-element.40) | copy-start | bytes 196612

commit v2 on v1

--- a/solution.py
+++ b/solution.py
@@ -20,7 +20,12 @@
 MIDDLE_SHORT = ((0, 384), (384, 256), (640, 384))
 X_CUTS = (LATE_SHORT, MIDDLE_SHORT)
 G_CUTS = (EARLY_SHORT, LATE_SHORT)
-BACK_CUTS = (MIDDLE_SHORT, EARLY_SHORT)
+BACK_CUTS = (
+    MIDDLE_SHORT,
+    ((0, 128), (128, 128), (256, 256)),
+    ((512, 256), (768, 128), (896, 128)),
+)
+HALVES = ((0, 512), (512, 512))
 
 
 def coordinate(dim):
@@ -166,6 +171,26 @@
 
 
 def main_kernel(
+    ids_hbm,
+    weights_hbm,
+    stream_hbm,
+    cot_hbm,
+    gate_in_hbm,
+    conv_gate_hbm,
+    conv_value_hbm,
+    taps_hbm,
+    w_out_hbm,
+    w_gate_hbm,
+    w_up_hbm,
+    w_down_hbm,
+    half_hbm,
+    gate_in_grad_hbm,
+    conv_gate_grad_hbm,
+    conv_value_grad_hbm,
+    out_block_hbm,
+    gate_w_hbm,
+    up_w_hbm,
+    down_w_hbm,
     ids_ref,
     weights_ref,
     stream_ref,
@@ -174,36 +199,19 @@
     conv_gate_ref,
     conv_value_ref,
     taps_ref,
-    w_out_hbm,
-    w_gate_hbm,
-    w_up_hbm,
-    w_down_hbm,
-    half_ref,
-    gate_in_grad_ref,
-    conv_gate_grad_ref,
-    conv_value_grad_ref,
-    out_block_ref,
-    x_hbm,
-    g_hbm,
-    hidden_hbm,
-    gate_hbm,
-    up_hbm,
     send,
     middle,
     full_x,
     full_g,
-    wg,
-    wu,
+    wgu,
     wd,
     w_out,
     silu_keep,
     slope_keep,
     hidden,
-    gate_grad,
-    up_grad,
-    shared,
+    both_grad,
     arrived,
-    rows_out,
+    staged,
     back,
     added_ref,
     hot_ref,
@@ -219,8 +227,12 @@
     halo,
     conv_sum_ref,
     mixer_out,
+    small,
+    out_block_ref,
+    input_sems,
     load_sems,
     save_sems,
+    small_sems,
     send_sems,
     recv_sems,
     local_sems,
@@ -235,15 +247,39 @@
     sp = lax.axis_index("sp")
     partner = (sp, 1 - tp)
     greet_all()
+    inputs = [
+        pltpu.make_async_copy(source, target, input_sems.at[k])
+        for k, (source, target) in enumerate(
+            (
+                (ids_hbm, ids_ref),
+                (weights_hbm, weights_ref),
+                (stream_hbm, stream_ref),
+                (cot_hbm, cot_ref),
+                (gate_in_hbm, gate_in_ref),
+                (conv_gate_hbm, conv_gate_ref),
+                (conv_value_hbm, conv_value_ref),
+                (taps_hbm, taps_ref),
+            )
+        )
+    ]
+    start_all(inputs)
     loads = [
         pltpu.make_async_copy(source, target, load_sems.at[k])
         for k, (source, target) in enumerate(
-            ((w_gate_hbm.at[0], wg), (w_up_hbm.at[0], wu), (w_down_hbm.at[0], wd), (w_out_hbm, w_out))
+            (
+                (w_gate_hbm.at[0], wgu.at[:, pl.ds(0, 512)]),
+                (w_up_hbm.at[0], wgu.at[:, pl.ds(512, 512)]),
+                (w_down_hbm.at[0], wd),
+                (w_out_hbm, w_out),
+            )
         )
     ]
     start_all(loads)
+    inputs[0].wait()
 
     slot0, slot1 = slots_in_lanes(ids_ref[...])
+    for copy in inputs[1:]:
+        copy.wait()
     weight0, weight1 = weights_ref[0:1, :], weights_ref[1:2, :]
 
     def row_numbers(place):
@@ -271,6 +307,7 @@
             )
 
     full = (full_x, full_g)
+    shared, rows_out = send.at[0], send.at[1]
 
     def stream_of(number, spots_of, cuts, chunk):
         portions = []
@@ -306,22 +343,22 @@
             chunk,
         )
 
-    def homeward(chunk):
+    def homeward(number):
         return stream_of(
-            4 + chunk,
+            4 + number,
             lambda cut: (
                 (rows_out, cut[0]),
                 (back.at[0], cut[0]),
                 (back.at[1], cut[0]),
                 (back.at[2], cut[0]),
             ),
-            BACK_CUTS[chunk],
-            chunk,
+            BACK_CUTS[number],
+            min(number, 1),
         )
 
     xs = [outward(0, chunk) for chunk in range(2)]
     gs = [outward(1, chunk) for chunk in range(2)]
-    backs = [homeward(chunk) for chunk in range(2)]
+    backs = [homeward(number) for number in range(3)]
 
     def begin(portions):
         for portion in portions:
@@ -351,16 +388,36 @@
         for crossing in crossings[tensor, chunk]:
             crossing.wait()
 
-    def save(source, target):
-        copy = pltpu.make_async_copy(source, target, save_sems.at[len(saves)])
-        copy.start()
-        saves.append(copy)
+    def weight_tile(number):
+        slot = number % 2
+        if number >= 2:
+            for copy in saves[number - 2]:
+                copy.wait()
+        if number < 4:
+            at = pl.ds(number * 512, 512)
+            columns = full_x[:, :, :, :, at].reshape(1024, 512)
+            staged[slot] = dot_tn(columns, both_grad[...]).astype(BF)
+            pairs = (
+                (staged.at[slot, :, pl.ds(0, 512)], gate_w_hbm.at[at]),
+                (staged.at[slot, :, pl.ds(512, 512)], up_w_hbm.at[at]),
+            )
+        else:
+            at = pl.ds((number - 4) * 1024, 1024)
+            columns = full_g[:, :, :, :, at].reshape(1024, 1024)
+            staged[slot] = dot_tn(hidden[...], columns).astype(BF)
+            pairs = ((staged.at[slot], down_w_hbm.at[:, at]),)
+        copies = [
+            pltpu.make_async_copy(source, target, save_sems.at[number, k])
+            for k, (source, target) in enumerate(pairs)
+        ]
+        start_all(copies)
+        saves.append(copies)
 
     def activate(chunk):
         rows = full_x[pl.ds(chunk * 2, 2)].reshape(512, 2048)
         at = pl.ds(chunk * 512, 512)
-        pre_gate = dot(rows, wg[...])
-        pre_up = dot(rows, wu[...])
+        pre_gate = dot(rows, wgu[:, 0:512])
+        pre_up = dot(rows, wgu[:, 512:1024])
         sigmoid = jax.nn.sigmoid(pre_gate)
         silu = pre_gate * sigmoid
         silu_keep[at, :] = silu
@@ -371,13 +428,13 @@
         rows = full_g[pl.ds(chunk * 2, 2)].reshape(512, 2048)
         at = pl.ds(chunk * 512, 512)
         hidden_grad = dot_nt(rows, wd[...])
-        up_grad[at, :] = (hidden_grad * silu_keep[at, :]).astype(BF)
-        gate_grad[at, :] = (hidden_grad * slope_keep[at, :]).astype(BF)
+        both_grad[at, 512:1024] = (hidden_grad * silu_keep[at, :]).astype(BF)
+        both_grad[at, 0:512] = (hidden_grad * slope_keep[at, :]).astype(BF)
 
     def partial_of(side, cut, chunk):
         at = pl.ds(pl.multiple_of(side * 1024 + cut[0], 128), cut[1])
         rows = pl.ds(chunk * 512, 512)
-        return dot_nt(gate_grad[rows, :], wg[at, :]) + dot_nt(up_grad[rows, :], wu[at, :])
+        return dot_nt(both_grad[rows, :], wgu[at, :])
 
     shares = {}
 
@@ -386,12 +443,12 @@
 
     def share_theirs(chunk):
         shares[chunk] = []
-        for which, cut in enumerate(BACK_CUTS[chunk]):
+        for which, cut in enumerate(HALVES):
             index = part(chunk, cut)
             shared[index] = (
                 partial_of(1 - tp, cut, chunk).astype(BF).reshape(2, 4, 4, SLOTS, cut[1])
             )
-            number = 12 + chunk * 3 + which
+            number = 12 + chunk * 2 + which
             share = remote(
                 shared.at[index],
                 arrived.at[index],
@@ -402,15 +459,15 @@
             share.start()
             shares[chunk].append(share)
 
-    def add_mine(chunk, begin_return):
-        for which, cut in enumerate(BACK_CUTS[chunk]):
+    def add_mine(chunk):
+        for which, cut in enumerate(HALVES):
             index = part(chunk, cut)
             mine = partial_of(tp, cut, chunk).astype(BF).astype(F32)
             shares[chunk][which].wait_recv()
             theirs = arrived[index].reshape(512, cut[1]).astype(F32)
             rows_out[index] = (mine + theirs).astype(BF).reshape(2, 4, 4, SLOTS, cut[1])
-            if begin_return:
-                start_phase(backs[chunk][which][0])
+            if chunk == 1:
+                begin(backs[1 + which])
 
     gather_x(0)
     all_greeted()
@@ -418,6 +475,7 @@
     gather_g(0)
     begin(gs[0])
     gather_x(1)
+    begin(xs[1])
     gather_g(1)
     pad_left[pl.ds(8, 256), :] = conv_gate_ref[...].astype(F32) * conv_value_ref[...].astype(F32)
     left = remote(
@@ -430,6 +488,7 @@
     left.start()
     advance(xs[0], 1)
     advance(gs[0], 1)
+    begin(gs[1])
     left.wait()
     pad_left[pl.ds(0, 8), :] = jnp.where(sp == 0, 0.0, halo[0])
     conv_sum = jnp.zeros((256, 512), F32)
@@ -439,64 +498,69 @@
     mixer_out[...] = (gate_in_ref[...].astype(F32) * conv_sum).astype(BF)
     advance(xs[0], 2)
     advance(gs[0], 2)
-    begin(xs[1])
+    advance(xs[1], 1)
+    advance(gs[1], 1)
     cross(0, 0)
-    begin(gs[1])
-    cross(1, 0)
     for load in loads:
         load.wait()
     crossed(0, 0)
+    cross(1, 0)
+    advance(xs[1], 2)
     activate(0)
-    advance(xs[1], 1)
     crossed(1, 0)
+    advance(gs[1], 2)
     differentiate(0)
-    advance(gs[1], 1)
+    for stream in (*xs, *gs):
+        for portion in stream:
+            sent_phase(portion[0])
     share_theirs(0)
-    advance(xs[1], 2)
-    add_mine(0, False)
-    advance(gs[1], 2)
+    add_mine(0)
     begin(backs[0])
     cross(0, 1)
     crossed(0, 1)
     activate(1)
-    save(full_x, x_hbm)
-    save(hidden, hidden_hbm)
+    cross(1, 1)
     advance(backs[0], 1)
-    cross(1, 1)
     crossed(1, 1)
     differentiate(1)
-    save(full_g, g_hbm)
-    save(gate_grad, gate_hbm)
-    save(up_grad, up_hbm)
     share_theirs(1)
+    add_mine(1)
     advance(backs[0], 2)
-    add_mine(1, True)
+    weight_tile(0)
     for portion in backs[0]:
         arrive_phase(portion[2])
     added_ref[...] = dot_tn(
         hot_ref[pl.ds(0, 512), :], back[2, pl.ds(0, 2)].reshape(512, 1024)
     ) + cot_ref[...].astype(F32)
     advance(backs[1], 1)
+    weight_tile(1)
+    advance(backs[2], 1)
+    weight_tile(2)
     advance(backs[1], 2)
-
+    weight_tile(3)
+    advance(backs[2], 2)
+    weight_tile(4)
     swaps = []
-    for which, portion in enumerate(backs[1]):
-        arrive_phase(portion[2])
-        cut = BACK_CUTS[1][which]
-        columns = pl.ds(*cut)
-        rows = back[2, pl.ds(2, 2), :, :, :, columns].reshape(512, cut[1])
-        total = (added_ref[:, columns] + dot_tn(hot_ref[pl.ds(512, 512), :], rows)).astype(BF)
-        half_ref[:, columns] = total
-        whole[tp, :, columns] = total
+
+    def combine(which):
+        for portion in backs[1 + which]:
+            arrive_phase(portion[2])
+        columns = pl.ds(*HALVES[which])
+        rows = back[2, pl.ds(2, 2), :, :, :, columns].reshape(512, 512)
+        total = added_ref[:, columns] + dot_tn(hot_ref[pl.ds(512, 512), :], rows)
+        whole[tp, :, columns] = total.astype(BF)
         swap = remote(
             whole.at[tp, :, columns],
             whole.at[tp, :, columns],
-            tp_send.at[18 + which],
-            tp_recv.at[18 + which],
+            tp_send.at[16 + which],
+            tp_recv.at[16 + which],
             partner,
         )
         swap.start()
         swaps.append(swap)
+
+    combine(0)
+    combine(1)
 
     def block_of(half):
         for part in range(2):
@@ -506,12 +570,7 @@
                     product[:, tile * 128 : (tile + 1) * 128].astype(BF).reshape(4, 4, 2, 16, 128)
                 )
 
-    block_of(tp)
-    for swap in swaps:
-        swap.wait()
-    block_of(1 - tp)
-
-    def fold_copies(which, phase):
+    def fold_copies(which, phase, half=None, late=0):
         start, count = UNIT_CUTS[which]
         dim = ORDERS[which][phase]
         here = coordinate(dim)
@@ -520,10 +579,14 @@
         for by in (2, 1, 3):
             index = [slice(None)] * len(left_dims)
             index[left_dims.index(dim)] = (here + by) % SIDE
+            kept = slice(None)
+            if half is not None:
+                kept = pl.ds(2 * half, 2)
+                index[0] = kept
             units = pl.ds(start, count)
             if phase == 0:
                 source = blocks.at[(*index, units)]
-                target = got1.at[by - 1, :, :, units]
+                target = got1.at[by - 1, kept, :, units]
             elif phase == 1:
                 source = sum1.at[(*index, units)]
                 target = got2.at[by - 1, :, units]
@@ -534,8 +597,8 @@
                 remote(
                     source,
                     target,
-                    fold_send.at[which, phase, by - 1],
-                    fold_recv.at[which, phase, by - 1],
+                    fold_send.at[which, phase + 3 * late, by - 1],
+                    fold_recv.at[which, phase + 3 * late, by - 1],
                     (peer_of(dim, by), tp),
                 )
             )
@@ -559,13 +622,34 @@
                 total = total + got3[by, units].astype(F32)
         return total
 
-    folds = [[fold_copies(which, phase) for phase in range(3)] for which in range(3)]
-    for fold in folds:
-        start_all(fold[0])
+    folds = [[[], fold_copies(which, 1), fold_copies(which, 2)] for which in range(3)]
+
+    def fold_first(which, half, late):
+        copies = fold_copies(which, 0, half, late)
+        start_all(copies)
+        folds[which][0] += copies
+
+    block_of(tp)
+    fold_first(0, tp, 0)
+    fold_first(1, tp, 0)
+    for swap in swaps:
+        swap.wait()
+    block_of(1 - tp)
+    fold_first(2, None, 0)
+    fold_first(0, 1 - tp, 1)
+    fold_first(1, 1 - tp, 1)
+    results = []
+
+    def deliver(source, target):
+        copy = pltpu.make_async_copy(source, target, small_sems.at[len(results)])
+        copy.start()
+        results.append(copy)
+
+    deliver(whole.at[tp], half_hbm)
 
     mixer_grad = (dot(whole[0], w_out[0:1024, :]) + dot(whole[1], w_out[1024:2048, :])).astype(BF)
     mixer_wide = mixer_grad.astype(F32)
-    gate_in_grad_ref[...] = (mixer_wide * conv_sum_ref[...]).astype(BF)
+    small[0] = (mixer_wide * conv_sum_ref[...]).astype(BF)
     pad_right[pl.ds(0, 256), :] = mixer_wide * gate_in_ref[...].astype(F32)
     right = remote(
         pad_right.at[pl.ds(0, 8)],
@@ -575,6 +659,8 @@
         ((sp + 63) % 64, tp),
     )
     right.start()
+    deliver(small.at[0], gate_in_grad_hbm)
+    weight_tile(5)
     for which, fold in enumerate(folds):
         start, count = UNIT_CUTS[which]
         for copy in fold[0]:
@@ -586,8 +672,10 @@
     prod_grad = jnp.zeros((256, 512), F32)
     for tap in range(3):
         prod_grad = prod_grad + taps_ref[tap : tap + 1, :] * pad_right[pl.ds(2 - tap, 256), :]
-    conv_gate_grad_ref[...] = (prod_grad * conv_value_ref[...].astype(F32)).astype(BF)
-    conv_value_grad_ref[...] = (prod_grad * conv_gate_ref[...].astype(F32)).astype(BF)
+    small[1] = (prod_grad * conv_value_ref[...].astype(F32)).astype(BF)
+    small[2] = (prod_grad * conv_gate_ref[...].astype(F32)).astype(BF)
+    deliver(small.at[1], conv_gate_grad_hbm)
+    deliver(small.at[2], conv_value_grad_hbm)
     for which, fold in enumerate(folds):
         start, count = UNIT_CUTS[which]
         for copy in fold[1]:
@@ -602,23 +690,30 @@
         for unit in range(count):
             tile, row = divmod(start + unit, 2)
             out_block_ref[pl.ds(row * 16, 16), pl.ds(tile * 128, 128)] = total[unit]
+    deliver(out_block_ref, out_block_hbm)
     for chunk in range(2):
         for share in shares[chunk]:
             share.wait_send()
-        for stream in (xs[chunk], gs[chunk], backs[chunk]):
+        for stream in (xs[chunk], gs[chunk]):
             for portion in stream:
-                for copies in portion:
+                for copies in portion[1:]:
                     sent_phase(copies)
+    for stream in backs:
+        for portion in stream:
+            for copies in portion:
+                sent_phase(copies)
     for fold in folds:
         for copies in fold:
             for copy in copies:
                 copy.wait_send()
-    for copy in saves:
+    for copy in results:
         copy.wait()
+    for copies in saves[4:]:
+        for copy in copies:
+            copy.wait()
 
 
 def main_call(*operands):
-    vmem = pl.BlockSpec(memory_space=pltpu.VMEM)
     hbm = pl.BlockSpec(memory_space=pl.ANY)
     shape = jax.ShapeDtypeStruct
     rows_shape = (4, 4, 4, SLOTS, 1024)
@@ -632,31 +727,34 @@
             shape((256, 512), BF),
             shape((256, 512), BF),
             shape((32, 512), F32),
-            shape(full_shape, BF),
-            shape(full_shape, BF),
-            shape((1024, 512), BF),
-            shape((1024, 512), BF),
-            shape((1024, 512), BF),
+            shape((2048, 512), BF),
+            shape((2048, 512), BF),
+            shape((512, 2048), BF),
         ),
-        in_specs=[vmem] * 8 + [hbm] * 4,
-        out_specs=(vmem,) * 5 + (hbm,) * 5,
+        in_specs=[hbm] * 12,
+        out_specs=(hbm,) * 8,
         scratch_shapes=[
+            pltpu.VMEM((2, 256), jnp.int32),
+            pltpu.VMEM((2, 256), F32),
+            pltpu.VMEM((256, 1024), BF),
+            pltpu.VMEM((256, 1024), BF),
+            pltpu.VMEM((256, 512), BF),
+            pltpu.VMEM((256, 512), BF),
+            pltpu.VMEM((256, 512), BF),
+            pltpu.VMEM((3, 512), F32),
             pltpu.VMEM((2, *rows_shape), BF),
             pltpu.VMEM((2, 2, *rows_shape), BF),
             pltpu.VMEM(full_shape, BF),
             pltpu.VMEM(full_shape, BF),
-            pltpu.VMEM((2048, 512), BF),
-            pltpu.VMEM((2048, 512), BF),
+            pltpu.VMEM((2048, 1024), BF),
             pltpu.VMEM((512, 2048), BF),
             pltpu.VMEM((2048, 512), BF),
             pltpu.VMEM((1024, 512), F32),
             pltpu.VMEM((1024, 512), F32),
             pltpu.VMEM((1024, 512), BF),
-            pltpu.VMEM((1024, 512), BF),
-            pltpu.VMEM((1024, 512), BF),
+            pltpu.VMEM((1024, 1024), BF),
             pltpu.VMEM(rows_shape, BF),
-            pltpu.VMEM(rows_shape, BF),
-            pltpu.VMEM(rows_shape, BF),
+            pltpu.VMEM((2, 512, 1024), BF),
             pltpu.VMEM((3, *rows_shape), BF),
             pltpu.VMEM((256, 1024), F32),
             pltpu.VMEM((1024, 256), BF),
@@ -672,22 +770,103 @@
             pltpu.VMEM((2, 8, 512), F32),
             pltpu.VMEM((256, 512), F32),
             pltpu.VMEM((256, 512), BF),
+            pltpu.VMEM((3, 256, 512), BF),
+            pltpu.VMEM((32, 512), F32),
+            dma((8,)),
             dma((4,)),
+            dma((6, 2)),
             dma((5,)),
-            dma((18, 3, 3)),
-            dma((18, 3, 3)),
-            dma((18, 3)),
-            dma((21,)),
-            dma((21,)),
+            dma((21, 3, 3)),
+            dma((21, 3, 3)),
+            dma((21, 3)),
+            dma((18,)),
+            dma((18,)),
             dma((2,)),
             dma((2,)),
-            dma((3, 3, 3)),
-            dma((3, 3, 3)),
+            dma((3, 4, 3)),
+            dma((3, 4, 3)),
         ],
         compiler_params=pltpu.CompilerParams(
             collective_id=0, has_side_effects=True, vmem_limit_bytes=67043328
         ),
     )(*operands)
+
+
+def finish_kernel(*refs):
+    sources, targets = refs[:8], refs[8:16]
+    passing, held, narrow, wide, in_sems, out_sems, big_in, big_out = (
+        refs[16:20],
+        refs[20],
+        refs[21:24],
+        refs[24:27],
+        *refs[27:31],
+    )
+    passing = (*passing, held)
+
+    def rows_of(which, step):
+        rows = narrow[which].shape[1]
+        return pl.ds(pl.multiple_of(step * rows, rows), rows)
+
+    def taken(which, step):
+        return pltpu.make_async_copy(
+            sources[5 + which].at[rows_of(which, step)],
+            narrow[which].at[step],
+            big_in.at[which, step],
+        )
+
+    def given(which, step):
+        return pltpu.make_async_copy(
+            wide[which].at[step],
+            targets[5 + which].at[0, rows_of(which, step)],
+            big_out.at[which, step],
+        )
+
+    ins = [
+        pltpu.make_async_copy(sources[k], passing[k], in_sems.at[k]) for k in range(5)
+    ]
+    outs = [
+        pltpu.make_async_copy(passing[k], targets[k], out_sems.at[k]) for k in range(5)
+    ]
+    for step in range(4):
+        for which in range(3):
+            taken(which, step).start()
+    start_all(ins)
+
+    def widen(step, carry):
+        for which in range(3):
+            taken(which, step).wait()
+            wide[which][step] = narrow[which][step].astype(F32)
+            given(which, step).start()
+        return carry
+
+    lax.fori_loop(0, 4, widen, 0)
+    for k in range(5):
+        ins[k].wait()
+        outs[k].start()
+    for step in range(4):
+        for which in range(3):
+            given(which, step).wait()
+    for copy in outs:
+        copy.wait()
+
+
+def finished(produced):
+    hbm = pl.BlockSpec(memory_space=pl.ANY)
+    dma = pltpu.SemaphoreType.DMA
+    shape = jax.ShapeDtypeStruct
+    tiles = ((4, 512, 512), (4, 512, 512), (4, 128, 2048))
+    return pl.pallas_call(
+        finish_kernel,
+        out_shape=tuple(shape(array.shape, array.dtype) for array in produced[:5])
+        + tuple(shape((1, *array.shape), F32) for array in produced[5:]),
+        in_specs=[hbm] * 8,
+        out_specs=(hbm,) * 8,
+        scratch_shapes=[pltpu.VMEM(array.shape, array.dtype) for array in produced[:5]]
+        + [pltpu.VMEM(tile, BF) for tile in tiles]
+        + [pltpu.VMEM(tile, F32) for tile in tiles]
+        + [dma((5,)), dma((5,)), dma((3, 4)), dma((3, 4))],
+        compiler_params=pltpu.CompilerParams(vmem_limit_bytes=67043328),
+    )(*produced)
 
 
 def shards(
@@ -704,7 +883,7 @@
     w_up,
     w_down,
 ):
-    half, gate_in_grad, conv_gate_grad, conv_value_grad, out_block, x, g, hidden, gate, up = main_call(
+    produced = main_call(
         route_ids.T,
         route_weights.T,
         stream,
@@ -718,18 +897,7 @@
         w_up,
         w_down,
     )
-    x = x.reshape(1024, 2048)
-    g = g.reshape(1024, 2048)
-    return (
-        half,
-        gate_in_grad,
-        conv_gate_grad,
-        conv_value_grad,
-        out_block,
-        dot_tn(x, gate)[None],
-        dot_tn(x, up)[None],
-        dot_tn(hidden, g)[None],
-    )
+    return finished(produced)
 
 
 def solution(mesh):

time: 141 us -> 123 us (0.87)
  matrix products: 15.9 us -> 0 us
  local copies, waits for them, and re-layouts: 3.57 us -> 0 us
    dot_general x3 -> x0, matrix products: 15.9 us -> none  [dot_tn(): lax.dot_general(a, b, (((0,), (0,)), ((), ())), preferred_element_type=F32)]
    pallas_call x0 -> x1, Pallas kernels: none -> 7.57 us  [finished(): pl.pallas_call(finish_kernel, out_shape=tuple((shape(array.shape, array.d...]
    pallas_call x1, Pallas kernels: 121 us -> 114 us  [main_call(): pl.pallas_call(main_kernel, out_shape=(shape((256, 1024), BF), shape((256...]
    unnamed x23 -> x0, local copies, waits for them, and re-layouts: 3.57 us -> none
where the time goes in v2:
time: 123 us
  Pallas kernels  122 us (99%)
    pallas_call x1, Pallas kernels, main_call(): pl.pallas_call(main_kernel, out_shape=(shape((256, 1024), BF), shape((256...  114 us
    pallas_call x1, Pallas kernels, finished(): pl.pallas_call(finish_kernel, out_shape=tuple((shape(array.shape, array.d...  7.57 us

profile of v2, /device:TPU:0, one launch (start us, length us, event | category | flops | bytes accessed | tf_op | source)
XLA Modules:
  0.0 122.6 jit_solution(1970142407710296070)
XLA Ops:
  0.6 114.2 %shard_map.179 = (bf16[256,1024]{1,0:T(8,128)(2,1)}, bf16[256,512]{1,0:T(8,128)(2,1)}, bf16[256,512]{1,0:T(8,128)(2,1)}, bf16[256,512]{1,0:T(8,128)(2,1)}, f32[3...) custom-call(s32[2,256]{1,0:T(2,128)} %bitcast.2, ...), custom_call_target="tpu_custom_call" | custom-call | tf_op jit(solution)/shard_map/pallas_call | solution.py:722
  114.9 7.6 %shard_map.180 = (bf16[256,1024]{1,0:T(8,128)(2,1)}, bf16[256,512]{1,0:T(8,128)(2,1)}, bf16[256,512]{1,0:T(8,128)(2,1)}, bf16[256,512]{1,0:T(8,128)(2,1)}, f32[3...) custom-call(bf16[256,1024]{1,0:T(8,128)(2,1)} %get-tuple-element.16.refs_0_, ...), custom_call_target="tpu_custom_call" | custom-call | tf_op jit(solution)/shard_map/pallas_call | solution.py:858

commit v3 on v2

--- a/solution.py
+++ b/solution.py
@@ -42,65 +42,67 @@
     return ref.at[(*index, slice(None), pl.ds(start, width))]
 
 
-def phase_copies(source, target, dim, width, chunk, send_sem, recv_sem, local_sem):
-    here = coordinate(dim)
-    tp = lax.axis_index("tp")
-    moves = []
-    if dim == 0:
+class Phase:
+    def __init__(self, source, target, dim, width, chunk, send_sem, recv_sem):
+        here = coordinate(dim)
+        tp = lax.axis_index("tp")
         every = (slice(None), slice(None))
-        if chunk == 0:
-            kept = ((0, *every), (0, *every))
-            moves.append((2, (1, *every), (1, *every)))
+        both = pl.ds(2 * chunk, 2)
+        moves = []
+        if dim == 0:
+            kept = None
+            if chunk == 0:
+                kept = (0, *every)
+                moves.append((2, (1, *every), (1, *every)))
+                gone = (1, *every)
+            else:
+                moves.append((1, (2, *every), (3, *every)))
+                moves.append((3, (3, *every), (2, *every)))
+                gone = (both, *every)
         else:
-            kept = None
-            moves.append((1, (2, *every), (3, *every)))
-            moves.append((3, (3, *every), (2, *every)))
-    else:
-
-        def at(place):
-            index = [pl.ds(2 * chunk, 2), slice(None), slice(None)]
-            index[dim] = place
-            return tuple(index)
-
-        kept = (at(here), at(here))
-        for by in (2, 1, 3):
-            moves.append((by, at((here + by) % SIDE), at(here)))
-    sent = [
-        pltpu.make_async_remote_copy(
-            src_ref=piece(source, from_index, width),
-            dst_ref=piece(target, to_index, width),
-            send_sem=send_sem.at[by - 1],
-            recv_sem=recv_sem.at[by - 1],
-            device_id=(peer_of(dim, by), tp),
-            device_id_type=MESH,
-        )
-        for by, from_index, to_index in moves
-    ]
-    local = []
-    if kept is not None:
-        local.append(
-            pltpu.make_async_copy(
-                piece(source, kept[0], width), piece(target, kept[1], width), local_sem
-            )
-        )
-    return sent, local
-
-
-def start_phase(copies):
-    for copy in copies[0] + copies[1]:
-        copy.start()
-
-
-def arrive_phase(copies):
-    for copy in copies[0]:
-        copy.wait_recv()
-    for copy in copies[1]:
-        copy.wait()
-
-
-def sent_phase(copies):
-    for copy in copies[0]:
-        copy.wait_send()
+
+            def at(place):
+                index = [both, slice(None), slice(None)]
+                index[dim] = place
+                return tuple(index)
+
+            kept = at(here)
+            for by in (2, 1, 3):
+                moves.append((by, at((here + by) % SIDE), at(here)))
+            gone = at(pl.ds(0, 3))
+        self.copies = [
+            pltpu.make_async_remote_copy(
+                src_ref=piece(source, from_index, width),
+                dst_ref=piece(target, to_index, width),
+                send_sem=send_sem,
+                recv_sem=recv_sem,
+                device_id=(peer_of(dim, by), tp),
+                device_id_type=MESH,
+            )
+            for by, from_index, to_index in moves
+        ]
+        if kept is not None:
+            self.copies.append(
+                pltpu.make_async_copy(
+                    piece(source, kept, width), piece(target, kept, width), recv_sem
+                )
+            )
+        filled = piece(target, (both, *every), width)
+        self.filled = pltpu.make_async_copy(filled, filled, recv_sem)
+        left = piece(source, gone, width)
+        self.left = pltpu.make_async_copy(left, left, send_sem)
+
+
+def start_phase(phase):
+    start_all(phase.copies)
+
+
+def arrive_phase(phase):
+    phase.filled.wait()
+
+
+def sent_phase(phase):
+    phase.left.wait()
 
 
 def start_all(copies):
@@ -235,7 +237,6 @@
     small_sems,
     send_sems,
     recv_sems,
-    local_sems,
     tp_send,
     tp_recv,
     halo_send,
@@ -315,7 +316,7 @@
             spots = spots_of(cut)
             portions.append(
                 [
-                    phase_copies(
+                    Phase(
                         spots[phase],
                         spots[phase + 1],
                         ORDERS[which][phase],
@@ -323,7 +324,6 @@
                         chunk,
                         send_sems.at[number * 3 + which, phase],
                         recv_sems.at[number * 3 + which, phase],
-                        local_sems.at[number * 3 + which, phase],
                     )
                     for phase in range(3)
                 ]
@@ -369,24 +369,25 @@
             arrive_phase(portion[phase - 1])
             start_phase(portion[phase])
 
-    crossings = {}
     saves = []
 
+    def half_of(tensor, chunk, cut):
+        start = pl.multiple_of(tp * 1024 + cut[0], 128)
+        return full[tensor].at[pl.ds(2 * chunk, 2), :, :, :, pl.ds(start, cut[1])]
+
+    def crossing(tensor, chunk, cut):
+        part = half_of(tensor, chunk, cut)
+        number = chunk * 2 + tensor
+        return remote(part, part, tp_send.at[number], tp_recv.at[number], partner)
+
     def cross(tensor, chunk):
-        crossings[tensor, chunk] = []
         portions = (xs, gs)[tensor][chunk]
         for which, cut in enumerate((X_CUTS, G_CUTS)[tensor][chunk]):
-            number = (chunk * 2 + tensor) * 3 + which
             arrive_phase(portions[which][2])
-            start = pl.multiple_of(tp * 1024 + cut[0], 128)
-            part = full[tensor].at[pl.ds(2 * chunk, 2), :, :, :, pl.ds(start, cut[1])]
-            crossing = remote(part, part, tp_send.at[number], tp_recv.at[number], partner)
-            crossing.start()
-            crossings[tensor, chunk].append(crossing)
+            crossing(tensor, chunk, cut).start()
 
     def crossed(tensor, chunk):
-        for crossing in crossings[tensor, chunk]:
-            crossing.wait()
+        crossing(tensor, chunk, (0, 1024)).wait()
 
     def weight_tile(number):
         slot = number % 2
@@ -448,7 +449,7 @@
             shared[index] = (
                 partial_of(1 - tp, cut, chunk).astype(BF).reshape(2, 4, 4, SLOTS, cut[1])
             )
-            number = 12 + chunk * 2 + which
+            number = 4 + chunk * 2 + which
             share = remote(
                 shared.at[index],
                 arrived.at[index],
@@ -518,23 +519,23 @@
     begin(backs[0])
     cross(0, 1)
     crossed(0, 1)
+    cross(1, 1)
     activate(1)
-    cross(1, 1)
-    advance(backs[0], 1)
     crossed(1, 1)
     differentiate(1)
+    advance(backs[0], 1)
     share_theirs(1)
     add_mine(1)
     advance(backs[0], 2)
     weight_tile(0)
+    advance(backs[1], 1)
+    weight_tile(1)
+    advance(backs[2], 1)
     for portion in backs[0]:
         arrive_phase(portion[2])
     added_ref[...] = dot_tn(
         hot_ref[pl.ds(0, 512), :], back[2, pl.ds(0, 2)].reshape(512, 1024)
     ) + cot_ref[...].astype(F32)
-    advance(backs[1], 1)
-    weight_tile(1)
-    advance(backs[2], 1)
     weight_tile(2)
     advance(backs[1], 2)
     weight_tile(3)
@@ -552,8 +553,8 @@
         swap = remote(
             whole.at[tp, :, columns],
             whole.at[tp, :, columns],
-            tp_send.at[16 + which],
-            tp_recv.at[16 + which],
+            tp_send.at[8 + which],
+            tp_recv.at[8 + which],
             partner,
         )
         swap.start()
@@ -597,12 +598,28 @@
                 remote(
                     source,
                     target,
-                    fold_send.at[which, phase + 3 * late, by - 1],
-                    fold_recv.at[which, phase + 3 * late, by - 1],
+                    fold_send.at[which, phase + 3 * late],
+                    fold_recv.at[which, phase + 3 * late],
                     (peer_of(dim, by), tp),
                 )
             )
-        return copies
+        index = [slice(None)] * len(left_dims)
+        index[left_dims.index(dim)] = pl.ds(0, 3)
+        kept = slice(None)
+        if half is not None:
+            kept = pl.ds(2 * half, 2)
+            index[0] = kept
+        if phase == 0:
+            source, target = blocks.at[(*index, units)], got1.at[:, kept, :, units]
+        elif phase == 1:
+            source, target = sum1.at[(*index, units)], got2.at[:, :, units]
+        else:
+            source, target = sum2.at[(*index, units)], got3.at[:, units]
+        ended = (
+            pltpu.make_async_copy(target, target, fold_recv.at[which, phase + 3 * late]),
+            pltpu.make_async_copy(source, source, fold_send.at[which, phase + 3 * late]),
+        )
+        return copies, ended
 
     def folded(which, phase):
         start, count = UNIT_CUTS[which]
@@ -622,12 +639,17 @@
                 total = total + got3[by, units].astype(F32)
         return total
 
-    folds = [[[], fold_copies(which, 1), fold_copies(which, 2)] for which in range(3)]
+    folds = [[[], [], []] for which in range(3)]
 
     def fold_first(which, half, late):
-        copies = fold_copies(which, 0, half, late)
+        copies, ended = fold_copies(which, 0, half, late)
         start_all(copies)
-        folds[which][0] += copies
+        folds[which][0].append(ended)
+
+    def fold_next(which, phase):
+        copies, ended = fold_copies(which, phase)
+        start_all(copies)
+        folds[which][phase].append(ended)
 
     block_of(tp)
     fold_first(0, tp, 0)
@@ -663,10 +685,10 @@
     weight_tile(5)
     for which, fold in enumerate(folds):
         start, count = UNIT_CUTS[which]
-        for copy in fold[0]:
-            copy.wait_recv()
+        for ended in fold[0]:
+            ended[0].wait()
         sum1[:, :, pl.ds(start, count)] = folded(which, 0).astype(BF)
-        start_all(fold[1])
+        fold_next(which, 1)
     right.wait()
     pad_right[pl.ds(256, 8), :] = jnp.where(sp == 63, 0.0, halo[1])
     prod_grad = jnp.zeros((256, 512), F32)
@@ -678,14 +700,14 @@
     deliver(small.at[2], conv_value_grad_hbm)
     for which, fold in enumerate(folds):
         start, count = UNIT_CUTS[which]
-        for copy in fold[1]:
-            copy.wait_recv()
+        for ended in fold[1]:
+            ended[0].wait()
         sum2[:, pl.ds(start, count)] = folded(which, 1).astype(BF)
-        start_all(fold[2])
+        fold_next(which, 2)
     for which, fold in enumerate(folds):
         start, count = UNIT_CUTS[which]
-        for copy in fold[2]:
-            copy.wait_recv()
+        for ended in fold[2]:
+            ended[0].wait()
         total = folded(which, 2)
         for unit in range(count):
             tile, row = divmod(start + unit, 2)
@@ -703,9 +725,9 @@
             for copies in portion:
                 sent_phase(copies)
     for fold in folds:
-        for copies in fold:
-            for copy in copies:
-                copy.wait_send()
+        for phase in fold:
+            for ended in phase:
+                ended[1].wait()
     for copy in results:
         copy.wait()
     for copies in saves[4:]:
@@ -776,15 +798,14 @@
             dma((4,)),
             dma((6, 2)),
             dma((5,)),
-            dma((21, 3, 3)),
-            dma((21, 3, 3)),
             dma((21, 3)),
-            dma((18,)),
-            dma((18,)),
+            dma((21, 3)),
+            dma((10,)),
+            dma((10,)),
             dma((2,)),
             dma((2,)),
-            dma((3, 4, 3)),
-            dma((3, 4, 3)),
+            dma((3, 4)),
+            dma((3, 4)),
         ],
         compiler_params=pltpu.CompilerParams(
             collective_id=0, has_side_effects=True, vmem_limit_bytes=67043328

time: 123 us -> 115 us (0.935)
  Pallas kernels: 122 us -> 114 us
    pallas_call x1, Pallas kernels: 114 us -> 107 us  [main_call(): pl.pallas_call(main_kernel, out_shape=(shape((256, 1024), BF), shape((256...]
where the time goes in v3:
time: 115 us
  Pallas kernels  114 us (99%)
    pallas_call x1, Pallas kernels, main_call(): pl.pallas_call(main_kernel, out_shape=(shape((256, 1024), BF), shape((256...  107 us
    pallas_call x1, Pallas kernels, finished(): pl.pallas_call(finish_kernel, out_shape=tuple((shape(array.shape, array.d...  7.57 us

profile of v3, /device:TPU:0, one launch (start us, length us, event | category | flops | bytes accessed | tf_op | source)
XLA Modules:
  0.0 115.0 jit_solution(17388432879919319822)
XLA Ops:
  0.6 106.6 %shard_map.179 = (bf16[256,1024]{1,0:T(8,128)(2,1)}, bf16[256,512]{1,0:T(8,128)(2,1)}, bf16[256,512]{1,0:T(8,128)(2,1)}, bf16[256,512]{1,0:T(8,128)(2,1)}, f32[3...) custom-call(s32[2,256]{1,0:T(2,128)} %bitcast.2, ...), custom_call_target="tpu_custom_call" | custom-call | tf_op jit(solution)/shard_map/pallas_call | solution.py:744
  107.3 7.6 %shard_map.180 = (bf16[256,1024]{1,0:T(8,128)(2,1)}, bf16[256,512]{1,0:T(8,128)(2,1)}, bf16[256,512]{1,0:T(8,128)(2,1)}, bf16[256,512]{1,0:T(8,128)(2,1)}, f32[3...) custom-call(bf16[256,1024]{1,0:T(8,128)(2,1)} %get-tuple-element.16.refs_0_, ...), custom_call_target="tpu_custom_call" | custom-call | tf_op jit(solution)/shard_map/pallas_call | solution.py:879

commit v4 on v3

--- a/solution.py
+++ b/solution.py
@@ -275,7 +275,6 @@
             )
         )
     ]
-    start_all(loads)
     inputs[0].wait()
 
     slot0, slot1 = slots_in_lanes(ids_ref[...])
@@ -472,6 +471,7 @@
 
     gather_x(0)
     all_greeted()
+    start_all(loads)
     begin(xs[0])
     gather_g(0)
     begin(gs[0])

time: 115 us -> 114 us (level)
    pallas_call x1, Pallas kernels: 107 us -> 105 us  [main_call(): pl.pallas_call(main_kernel, out_shape=(shape((256, 1024), BF), shape((256...]
where the time goes in v4:
time: 114 us
  Pallas kernels  113 us (99%)
    pallas_call x1, Pallas kernels, main_call(): pl.pallas_call(main_kernel, out_shape=(shape((256, 1024), BF), shape((256...  105 us
    pallas_call x1, Pallas kernels, finished(): pl.pallas_call(finish_kernel, out_shape=tuple((shape(array.shape, array.d...  7.57 us

profile of v4, /device:TPU:0, one launch (start us, length us, event | category | flops | bytes accessed | tf_op | source)
XLA Modules:
  0.0 113.6 jit_solution(6888979929626340818)
XLA Ops:
  0.6 105.2 %shard_map.179 = (bf16[256,1024]{1,0:T(8,128)(2,1)}, bf16[256,512]{1,0:T(8,128)(2,1)}, bf16[256,512]{1,0:T(8,128)(2,1)}, bf16[256,512]{1,0:T(8,128)(2,1)}, f32[3...) custom-call(s32[2,256]{1,0:T(2,128)} %bitcast.2, ...), custom_call_target="tpu_custom_call" | custom-call | tf_op jit(solution)/shard_map/pallas_call | solution.py:744
  105.9 7.6 %shard_map.180 = (bf16[256,1024]{1,0:T(8,128)(2,1)}, bf16[256,512]{1,0:T(8,128)(2,1)}, bf16[256,512]{1,0:T(8,128)(2,1)}, bf16[256,512]{1,0:T(8,128)(2,1)}, f32[3...) custom-call(bf16[256,1024]{1,0:T(8,128)(2,1)} %get-tuple-element.16.refs_0_, ...), custom_call_target="tpu_custom_call" | custom-call | tf_op jit(solution)/shard_map/pallas_call | solution.py:879

commit v5 on v4

--- a/solution.py
+++ b/solution.py
@@ -531,14 +531,14 @@
     advance(backs[1], 1)
     weight_tile(1)
     advance(backs[2], 1)
+    weight_tile(2)
+    weight_tile(3)
+    advance(backs[1], 2)
     for portion in backs[0]:
         arrive_phase(portion[2])
     added_ref[...] = dot_tn(
         hot_ref[pl.ds(0, 512), :], back[2, pl.ds(0, 2)].reshape(512, 1024)
     ) + cot_ref[...].astype(F32)
-    weight_tile(2)
-    advance(backs[1], 2)
-    weight_tile(3)
     advance(backs[2], 2)
     weight_tile(4)
     swaps = []
@@ -848,7 +848,7 @@
     outs = [
         pltpu.make_async_copy(passing[k], targets[k], out_sems.at[k]) for k in range(5)
     ]
-    for step in range(4):
+    for step in range(2):
         for which in range(3):
             taken(which, step).start()
     start_all(ins)
@@ -860,11 +860,11 @@
             given(which, step).start()
         return carry
 
-    lax.fori_loop(0, 4, widen, 0)
+    lax.fori_loop(0, 2, widen, 0)
     for k in range(5):
         ins[k].wait()
         outs[k].start()
-    for step in range(4):
+    for step in range(2):
         for which in range(3):
             given(which, step).wait()
     for copy in outs:
@@ -875,7 +875,7 @@
     hbm = pl.BlockSpec(memory_space=pl.ANY)
     dma = pltpu.SemaphoreType.DMA
     shape = jax.ShapeDtypeStruct
-    tiles = ((4, 512, 512), (4, 512, 512), (4, 128, 2048))
+    tiles = ((2, 1024, 512), (2, 1024, 512), (2, 256, 2048))
     return pl.pallas_call(
         finish_kernel,
         out_shape=tuple(shape(array.shape, array.dtype) for array in produced[:5])

time: 114 us -> 113 us (level)
  no operation moved by 1% of the time
where the time goes in v5:
time: 113 us
  Pallas kernels  112 us (99%)
    pallas_call x1, Pallas kernels, main_call(): pl.pallas_call(main_kernel, out_shape=(shape((256, 1024), BF), shape((256...  105 us
    pallas_call x1, Pallas kernels, finished(): pl.pallas_call(finish_kernel, out_shape=tuple((shape(array.shape, array.d...  7.41 us

profile of v5, /device:TPU:0, one launch (start us, length us, event | category | flops | bytes accessed | tf_op | source)
XLA Modules:
  0.0 113.2 jit_solution(9616850481990265842)
XLA Ops:
  0.6 105.0 %shard_map.179 = (bf16[256,1024]{1,0:T(8,128)(2,1)}, bf16[256,512]{1,0:T(8,128)(2,1)}, bf16[256,512]{1,0:T(8,128)(2,1)}, bf16[256,512]{1,0:T(8,128)(2,1)}, f32[3...) custom-call(s32[2,256]{1,0:T(2,128)} %bitcast.2, ...), custom_call_target="tpu_custom_call" | custom-call | tf_op jit(solution)/shard_map/pallas_call | solution.py:744
  105.7 7.4 %shard_map.180 = (bf16[256,1024]{1,0:T(8,128)(2,1)}, bf16[256,512]{1,0:T(8,128)(2,1)}, bf16[256,512]{1,0:T(8,128)(2,1)}, bf16[256,512]{1,0:T(8,128)(2,1)}, f32[3...) custom-call(bf16[256,1024]{1,0:T(8,128)(2,1)} %get-tuple-element.16.refs_0_, ...), custom_call_target="tpu_custom_call" | custom-call | tf_op jit(solution)/shard_map/pallas_call | solution.py:879
